TPU v7x, 512 devices: a whole 4x4x16 slice. The times are simulated.
512 devices in a mesh: sp: 64 (over z, y), tp: 8 (over x, core).
Axes of the slice: x: 4, y: 4, z: 16, core: 2. Of those that a mesh axis runs over, the one named last changes fastest.
Arguments:
- stream: bfloat16 [24576, 2048], P('sp'), may hold values from -40 to 40
- query_rows: bfloat16 [24576, 1024], P('sp', 'tp'), may hold values from -10 to 10
- key_rows: bfloat16 [24576, 256], P('sp'), may hold values from -10 to 10
- value_rows: bfloat16 [24576, 256], P('sp'), may hold values from -6 to 6
- doc_ids: int32 [24576], P('sp'), may hold values from 0 to 31, never falling along the last dimension, each value on 1 to 1536 neighbouring positions
- sink_logit: float32 [8], P('tp'), may hold values from 2 to 7
- out_weight: bfloat16 [1024, 2048], P('tp'), may hold values from -1.5 to 1.5
- norm_gain: float32 [2048], replicated, may hold values from 0.1 to 1.9
- gate_weight: bfloat16 [2048, 5632], P('sp', 'tp'), may hold values from -0.125 to 0.125
- up_weight: bfloat16 [2048, 5632], P('sp', 'tp'), may hold values from -0.125 to 0.125
- down_weight: bfloat16 [5632, 2048], P('tp', 'sp'), may hold values from -0.078125 to 0.078125
Outputs:
- mixed_out: bfloat16 [24576, 2048], P('sp')
Inputs may be any that keep to these rules, and one draw needn't show every extreme that they name: `doc_ids`: document numbers never fall along the sequence; each document has 1 to 1536 positions.
All inputs are finite; a program needn't handle non-finite values.
Results may differ from a plain program's by a relative error of at most 0.009.
Values may be sent and summed in bfloat16 or wider, within the bound.
A program may use at most 64 MiB of HBM per device.

v0:
```python
import jax
import jax.numpy as jnp
from jax import lax
from jax.sharding import Mesh
from jax.sharding import PartitionSpec as P

HEADS = 8
KVH = 2
HD = 128
WIN = 128
SP = ("sp_0", "sp_1")


norm_eps = 1e-06
masked_low = -1e30


def extended(value, sides, width):
    for axis, dim in sides:
        peers, length = (lax.axis_size(axis), value.shape[dim])
        up = [(i, (i + 1) % peers) for i in range(peers - 1)]
        down = [(j, i) for i, j in up]
        last = lax.slice_in_dim(value, length - width, length, axis=dim)
        initial = lax.slice_in_dim(value, 0, width, axis=dim)
        before = lax.ppermute(last, axis, up)
        after = lax.ppermute(initial, axis, down)
        value = jnp.concatenate([before, value, after], axis=dim)
    return value


def in_blocks(value, dim, peers):
    shape = value.shape
    tiles = value.reshape(*shape[:dim], peers, shape[dim] // peers, *shape[dim + 1 :])
    return jnp.moveaxis(tiles, dim, 0)


def sum_at_owner(value, axis, dim):
    tiles = in_blocks(value, dim, lax.axis_size(axis))
    arrived = lax.all_to_all(tiles, axis, split_axis=0, concat_axis=0, tiled=True)
    return arrived.astype(jnp.float32).sum(axis=0)


def sent_to_all(value, axis):
    peers = lax.axis_size(axis)
    return lax.all_to_all(
        jnp.broadcast_to(value[None], (peers, *value.shape)), axis, 0, 0, tiled=True
    )


def over_copies(value, axis):
    return sent_to_all(value, axis).sum(axis=0)


def joined_along(tiles, dim):
    shape = list(tiles.shape[1:])
    shape[dim] *= tiles.shape[0]
    return jnp.moveaxis(tiles, 0, dim).reshape(shape)


def gather_directly(value, axis, dim):
    tiles = sent_to_all(value, axis)
    return joined_along(tiles, dim)


def sent_together(arrays, axis, dim, along):
    both = jnp.concatenate(arrays, axis=along)
    whole, at, outs = (lax.all_gather(both, axis, axis=dim, tiled=True), 0, [])
    for a in arrays:
        outs.append(lax.slice_in_dim(whole, at, at + a.shape[along], axis=along))
        at += a.shape[along]
    return tuple(outs)


def gather_axes(value, axes, dim):
    for axis in reversed(axes):
        value = lax.all_gather(value, axis, axis=dim, tiled=True)
    return value


def per_device(
    stream,
    query_rows,
    key_rows,
    value_rows,
    doc_ids,
    sink_logit,
    out_weight,
    norm_gain,
    gate_weight,
    up_weight,
    down_weight,
):
    row_count = stream.shape[0]
    width_all = stream.shape[1]
    heads_here = query_rows.shape[1] // HD
    group_share = HEADS // KVH
    groups_here = max(1, heads_here // group_share)
    per_group = heads_here // groups_here
    tp_place = lax.axis_index("tp")
    group_first = tp_place * heads_here // group_share
    keys_here = lax.dynamic_slice_in_dim(key_rows, group_first * HD, groups_here * HD, 1)
    values_here = lax.dynamic_slice_in_dim(value_rows, group_first * HD, groups_here * HD, 1)
    keys_wide, values_wide, docs_wide = (
        extended(keys_here, ((SP, 0),), WIN),
        extended(values_here, ((SP, 0),), WIN),
        extended(doc_ids, ((SP, 0),), WIN),
    )
    seq_offset = lax.axis_index(SP) * row_count
    seq_total = row_count * lax.axis_size(SP)
    query_pos = seq_offset + jnp.arange(row_count, dtype=jnp.int32)
    key_pos = seq_offset - WIN + jnp.arange(row_count + 2 * WIN, dtype=jnp.int32)
    allowed = (
        (jnp.abs(query_pos[:, None] - key_pos[None, :]) <= WIN)
        & (key_pos[None, :] >= 0)
        & (key_pos[None, :] < seq_total)
        & (doc_ids[:, None] == docs_wide[None, :])
    )
    queries = query_rows.reshape(row_count, groups_here, per_group, HD)
    keys_grid = keys_wide.reshape(row_count + 2 * WIN, groups_here, HD)
    values_grid = values_wide.reshape(row_count + 2 * WIN, groups_here, HD)
    scores = jnp.einsum(
        "qgrd,kgd->grqk", queries, keys_grid, preferred_element_type=jnp.float32
    ) * HD ** (-0.5)
    masked = jnp.where(allowed[None, None], scores, masked_low)
    sinks = sink_logit.reshape(groups_here, per_group, 1, 1)
    peak = jnp.maximum(jnp.max(masked, axis=-1, keepdims=True), sinks)
    lifted = jnp.where(allowed[None, None], jnp.exp(masked - peak), 0.0)
    denom = jnp.sum(lifted, axis=-1, keepdims=True) + jnp.exp(sinks - peak)
    probs = (lifted / denom).astype(jnp.bfloat16)
    attended = jnp.einsum("grqk,kgd->qgrd", probs, values_grid, preferred_element_type=jnp.float32)
    attended = attended.astype(jnp.bfloat16).reshape(row_count, heads_here * HD)
    partial_value = jnp.dot(attended, out_weight, preferred_element_type=jnp.float32)
    columns = width_all // lax.axis_size("tp")
    begin_at = tp_place * columns
    branch = sum_at_owner(partial_value.astype(jnp.bfloat16), "tp", 1).astype(jnp.bfloat16)
    stream_part = lax.dynamic_slice_in_dim(stream, begin_at, columns, 1)
    carried = (stream_part.astype(jnp.float32) + branch.astype(jnp.float32)).astype(jnp.bfloat16)
    carried_f = carried.astype(jnp.float32)
    squares = over_copies(jnp.sum(carried_f * carried_f, axis=1), "tp")
    gain_part = lax.dynamic_slice_in_dim(norm_gain, begin_at, columns, 0)
    normed_part = (
        carried_f * lax.rsqrt(squares / width_all + norm_eps)[:, None] * gain_part[None, :]
    ).astype(jnp.bfloat16)
    normed = gather_directly(normed_part, "tp", 1)

    def add_rows(weight_rows):
        return jnp.dot(normed, weight_rows, preferred_element_type=jnp.float32)

    weight_pair = sent_together((gate_weight, up_weight), SP, 0, 1)
    gate_acc = add_rows(weight_pair[0])
    up_acc = add_rows(weight_pair[1])
    hidden = (jax.nn.silu(gate_acc) * up_acc).astype(jnp.bfloat16)
    terms = jnp.dot(hidden, gather_axes(down_weight, SP, 1), preferred_element_type=jnp.float32)
    feed = sum_at_owner(terms.astype(jnp.bfloat16), "tp", 1).astype(jnp.bfloat16)
    out_part = (carried_f + 0.5 * feed.astype(jnp.float32)).astype(jnp.bfloat16)
    return gather_directly(out_part, "tp", 1)


def solution(mesh):
    split = Mesh(mesh.devices.reshape(16, 4, mesh.shape["tp"]), ("sp_0", "sp_1", "tp"))
    placed = (
        P(SP, None),
        P(SP, "tp"),
        P(SP, None),
        P(SP, None),
        P(SP),
        P("tp"),
        P("tp", None),
        P(),
        P(SP, "tp"),
        P(SP, "tp"),
        P("tp", SP),
    )
    return jax.shard_map(
        per_device, mesh=split, in_specs=placed, out_specs=P(SP, None), check_vma=False
    )
```

profile of v0, /device:TPU:1, one launch (start us, length us, event | category | flops | bytes accessed | tf_op | source)
XLA Modules:
  0.0 308.2 jit_solution(575160341500205505)
XLA Ops:
  6.5 1.6 pad_maximum_fusion
  9.0 4.0 %collective-permute-start.2 = (s32[128]{0:T(128)S(1)}, s32[128]{0:T(128)S(1)}, u32[]{:S(2)}, u32[]{:S(2)}) collective-permute-start(s32[128]{0:T(128)S(1)} %get-tuple-element.11), channel_id=1, source_target_pairs={{0,8},{8,16},{16,24},{24,32},{32,40},{40,48},{48,56},{56,64},{64,7... | collective-permute-start | bytes 1544 | tf_op jit(solution)/shard_map/ppermute | solution.py:25
  13.0 1.3 collective-permute-start.3
  15.1 4.0 %collective-permute-start.4 = (bf16[128,128]{1,0:T(8,128)(2,1)S(1)}, bf16[128,128]{1,0:T(8,128)(2,1)S(1)}, u32[]{:S(2)}, u32[]{:S(2)}) collective-permute-start(bf16[128,128]{1,0:T(8,128)(2,1)S(1)} %get-tuple-element.9), channel_id=1, source_target_pairs={{0,8},{8,16},{16,24},{24,32},{32,40},{40,48},{48,56},{56,64},{64,7... | collective-permute-start | bytes 98312 | tf_op jit(solution)/shard_map/ppermute | solution.py:25
  19.1 1.3 collective-permute-start.5
  21.2 4.0 %collective-permute-start = (bf16[128,128]{1,0:T(8,128)(2,1)S(1)}, bf16[128,128]{1,0:T(8,128)(2,1)S(1)}, u32[]{:S(2)}, u32[]{:S(2)}) collective-permute-start(bf16[128,128]{1,0:T(8,128)(2,1)S(1)} %get-tuple-element.7), channel_id=1, source_target_pairs={{0,8},{8,16},{16,24},{24,32},{32,40},{40,48},{48,56},{56,64},{64,7... | collective-permute-start | bytes 98312 | tf_op jit(solution)/shard_map/ppermute | solution.py:25
  25.2 16.7 %all_gather.10 = bf16[704,128]{0,1:T(8,128)(2,1)} all-gather(bf16[704,32]{0,1:T(8,128)(2,1)} %param.21), channel_id=1, replica_groups=mesh['sp_0'=16,'sp_1'=4,'tp'=8] {'sp_1'}, dimensions={1}, use_global_device_ids=true | all-gather | bytes 225280 | tf_op jit(solution)/shard_map/all_gather | solution.py:76
  43.6 1.3 collective-permute-start.1
  45.6 1.5 fusion.58
  48.6 1.4 convolution_convert_fusion.1
  51.3 9.1 %all-to-all-start = ((bf16[8,384,256]{2,1,0:T(8,128)(2,1)}), bf16[8,384,256]{2,1,0:T(8,128)(2,1)S(1)}, u32[]{:S(2)}, u32[]{:S(2)}) async-start(bf16[8,384,256]{2,1,0:T(8,128)(2,1)} %bitcast.46), calls=%async_computation | async-start | bytes 3145728 | tf_op jit(solution)/shard_map/all_to_all | solution.py:39
  60.3 20.6 %all-to-all-done = bf16[8,384,256]{2,1,0:T(8,128)(2,1)S(1)} async-done(((bf16[8,384,256]{2,1,0:T(8,128)(2,1)}), bf16[8,384,256]{2,1,0:T(8,128)(2,1)S(1)}, u32[]{:S(2)}, u32[]{:S(2)}) %all-to-all-start) | async-done | bytes 1572896 | tf_op jit(solution)/shard_map/all_to_all | solution.py:39
  82.9 4.2 %all-to-all-start.1 = ((f32[8,1,384]{2,1,0:T(1,128)}), f32[8,1,384]{2,1,0:T(1,128)S(1)}, u32[]{:S(2)}, u32[]{:S(2)}) async-start(f32[8,1,384]{2,1,0:T(1,128)} %broadcast_in_dim.15), calls=%async_computation.1 | async-start | bytes 24576 | tf_op jit(solution)/shard_map/all_to_all | solution.py:45
  87.8 3.9 %all-to-all-done.1 = f32[8,1,384]{2,1,0:T(1,128)S(1)} async-done(((f32[8,1,384]{2,1,0:T(1,128)}), f32[8,1,384]{2,1,0:T(1,128)S(1)}, u32[]{:S(2)}, u32[]{:S(2)}) %all-to-all-start.1) | async-done | bytes 12320 | tf_op jit(solution)/shard_map/all_to_all | solution.py:45
  92.2 23.7 %all_to_all.26 = bf16[8,384,256]{1,2,0:T(8,128)(2,1)S(1)} all-to-all(bf16[8,384,256]{1,2,0:T(8,128)(2,1)S(1)} %broadcast_in_dim.16), channel_id=1, replica_groups=mesh['sp_0'=16,'sp_1'=4,'tp'=8] {'tp'}, dimensions={0} | all-to-all | bytes 3145728 | tf_op jit(solution)/shard_map/all_to_all | solution.py:45
  116.0 41.0 %all-gather.3.cloned.1.call-done = bf16[2048,1408]{1,0:T(8,128)(2,1)} async-done(((bf16[32,1408]{1,0:T(8,128)(2,1)}), bf16[2048,1408]{1,0:T(8,128)(2,1)}) %all-gather.3.cloned.1.call-update) | async-done | bytes 5767184 | tf_op jit(solution)/shard_map/all_gather | solution.py:67
  156.9 3.6 %fusion.2 = f32[384,704]{0,1:T(8,128)S(1)} fusion(bf16[384,2048]{0,1:T(8,128)(2,1)S(1)} %bitcast.49, bf16[2048,1408]{1,0:T(8,128)(2,1)} %all-gather.3.cloned.1.call-done), kind=kOutput, calls=%fused_computation.2 | convolution fusion | flops 1107296256 | bytes 5799936 | tf_op jit(solution)/shard_map/dot_general | solution.py:147
  160.5 68.3 %all-gather.5.cloned.1.call-done = bf16[704,2048]{0,1:T(8,128)(2,1)} async-done(((bf16[704,128]{0,1:T(8,128)(2,1)}), bf16[704,2048]{0,1:T(8,128)(2,1)}) %all-gather.5.cloned.1.call-update) | async-done | bytes 2883600 | tf_op jit(solution)/shard_map/all_gather | solution.py:76
  228.8 8.2 %convolution_convert_fusion = bf16[384,2048]{1,0:T(8,128)(2,1)} fusion(bf16[704,2048]{0,1:T(8,128)(2,1)} %all-gather.5.cloned.1.call-done, bf16[384,2048]{0,1:T(8,128)(2,1)S(1)} %bitcast.50, bf16[2048,1408]{1,0:T(8,128)(2,1)} %all-gather.3.cloned.1.call-done, f32[384,704]{0,1:T(8,128)S(1)} %fusion.2), kind=kOutput, calls=%fused_computation.4 | convolution fusion | flops 2217000960 | bytes 10518528 | tf_op jit(solution)/shard_map/dot_general | solution.py:153
  237.0 1.5 copy.37
  238.5 34.2 %all_to_all.27 = bf16[8,384,256]{2,1,0:T(8,128)(2,1)S(1)} all-to-all(bf16[8,384,256]{2,1,0:T(8,128)(2,1)S(1)} %bitcast.47), channel_id=1, replica_groups=mesh['sp_0'=16,'sp_1'=4,'tp'=8] {'tp'}, dimensions={0} | all-to-all | bytes 3145728 | tf_op jit(solution)/shard_map/all_to_all | solution.py:39
  273.2 24.0 %all_to_all.28 = bf16[8,384,256]{2,1,0:T(8,128)(2,1)S(1)} all-to-all(bf16[8,384,256]{2,1,0:T(8,128)(2,1)S(1)} %broadcast_in_dim.17), channel_id=1, replica_groups=mesh['sp_0'=16,'sp_1'=4,'tp'=8] {'tp'}, dimensions={0} | all-to-all | bytes 3145728 | tf_op jit(solution)/shard_map/all_to_all | solution.py:45
  297.2 1.6 copy.30
  298.8 2.6 copy.31
  (38 shorter events, 10.5 us)
Async XLA Ops:
  6.5 42.1 %copy-start = (bf16[128,2048]{1,0:T(8,128)(2,1)S(1)}, bf16[128,2048]{1,0:T(8,128)(2,1)}, u32[]{:S(2)}) copy-start(bf16[128,2048]{1,0:T(8,128)(2,1)} %param.17) | copy-start | bytes 1572868
  6.5 150.4 %all-gather.3.cloned.1.call-start = ((), (), s32[]{:S(2)}) async-start(), calls=%async_computation.5 | async-start | bytes 5857280 | tf_op jit(solution)/shard_map/all_gather | solution.py:67
  8.2 220.7 %all-gather.5.cloned.1.call-start = ((), (), s32[]{:S(2)}) async-start(), calls=%async_computation.6 | async-start | bytes 3342336 | tf_op jit(solution)/shard_map/all_gather | solution.py:76
  9.0 34.6 %collective-permute-start.2 = (s32[128]{0:T(128)S(1)}, s32[128]{0:T(128)S(1)}, u32[]{:S(2)}, u32[]{:S(2)}) collective-permute-start(s32[128]{0:T(128)S(1)} %get-tuple-element.11), channel_id=1, source_target_pairs={{0,8},{8,16},{16,24},{24,32},{32,40},{40,48},{48,56},{56,64},{64,7... | collective-permute-start | bytes 1544 | tf_op jit(solution)/shard_map/ppermute | solution.py:25
  13.0 31.9 %collective-permute-start.3 = (s32[128]{0:T(128)S(1)}, s32[128]{0:T(128)S(1)}, u32[]{:S(2)}, u32[]{:S(2)}) collective-permute-start(s32[128]{0:T(128)S(1)} %get-tuple-element.12), channel_id=1, source_target_pairs={{8,0},{16,8},{24,16},{32,24},{40,32},{48,40},{56,48},{64,56},{72,6... | collective-permute-start | bytes 1544 | tf_op jit(solution)/shard_map/ppermute | solution.py:26
  15.1 30.5 %collective-permute-start.4 = (bf16[128,128]{1,0:T(8,128)(2,1)S(1)}, bf16[128,128]{1,0:T(8,128)(2,1)S(1)}, u32[]{:S(2)}, u32[]{:S(2)}) collective-permute-start(bf16[128,128]{1,0:T(8,128)(2,1)S(1)} %get-tuple-element.9), channel_id=1, source_target_pairs={{0,8},{8,16},{16,24},{24,32},{32,40},{40,48},{48,56},{56,64},{64,7... | collective-permute-start | bytes 98312 | tf_op jit(solution)/shard_map/ppermute | solution.py:25
  19.1 26.5 %collective-permute-start.5 = (bf16[128,128]{1,0:T(8,128)(2,1)S(1)}, bf16[128,128]{1,0:T(8,128)(2,1)S(1)}, u32[]{:S(2)}, u32[]{:S(2)}) collective-permute-start(bf16[128,128]{1,0:T(8,128)(2,1)S(1)} %get-tuple-element.10), channel_id=1, source_target_pairs={{8,0},{16,8},{24,16},{32,24},{40,32},{48,40},{56,48},{64,56},{72,6... | collective-permute-start | bytes 98312 | tf_op jit(solution)/shard_map/ppermute | solution.py:26
  21.2 26.8 %collective-permute-start = (bf16[128,128]{1,0:T(8,128)(2,1)S(1)}, bf16[128,128]{1,0:T(8,128)(2,1)S(1)}, u32[]{:S(2)}, u32[]{:S(2)}) collective-permute-start(bf16[128,128]{1,0:T(8,128)(2,1)S(1)} %get-tuple-element.7), channel_id=1, source_target_pairs={{0,8},{8,16},{16,24},{24,32},{32,40},{40,48},{48,56},{56,64},{64,7... | collective-permute-start | bytes 98312 | tf_op jit(solution)/shard_map/ppermute | solution.py:25
  42.8 4.3 %copy-start.1 = (s32[384]{0:T(512)S(1)}, s32[384]{0:T(512)}, u32[]{:S(2)}) copy-start(s32[384]{0:T(512)} %param.15) | copy-start | bytes 4612
  43.6 5.1 %collective-permute-start.1 = (bf16[128,128]{1,0:T(8,128)(2,1)S(1)}, bf16[128,128]{1,0:T(8,128)(2,1)S(1)}, u32[]{:S(2)}, u32[]{:S(2)}) collective-permute-start(bf16[128,128]{1,0:T(8,128)(2,1)S(1)} %get-tuple-element.8), channel_id=1, source_target_pairs={{8,0},{16,8},{24,16},{32,24},{40,32},{48,40},{56,48},{64,56},{72,6... | collective-permute-start | bytes 98312 | tf_op jit(solution)/shard_map/ppermute | solution.py:26
  51.3 29.6 %all-to-all-start = ((bf16[8,384,256]{2,1,0:T(8,128)(2,1)}), bf16[8,384,256]{2,1,0:T(8,128)(2,1)S(1)}, u32[]{:S(2)}, u32[]{:S(2)}) async-start(bf16[8,384,256]{2,1,0:T(8,128)(2,1)} %bitcast.46), calls=%async_computation | async-start | bytes 3145728 | tf_op jit(solution)/shard_map/all_to_all | solution.py:39
  82.9 8.9 %all-to-all-start.1 = ((f32[8,1,384]{2,1,0:T(1,128)}), f32[8,1,384]{2,1,0:T(1,128)S(1)}, u32[]{:S(2)}, u32[]{:S(2)}) async-start(f32[8,1,384]{2,1,0:T(1,128)} %broadcast_in_dim.15), calls=%async_computation.1 | async-start | bytes 24576 | tf_op jit(solution)/shard_map/all_to_all | solution.py:45
Sparse Core Ops, SparseCore 0:
  10.3 146.6 all-gather.2
  159.0 69.7 all-gather.4
where the time goes:
time: 309 us; the launch traced here: 308 us
  waiting for transfers between devices  134 us (43%)
  blocking collectives  98.6 us (32%)
  starting transfers between devices  29.1 us (9%)
  matrix products  14.7 us (5%)
  between operations  14.3 us (5%)
  local copies, waits for them, and re-layouts  12 us (4%)
  other arithmetic  4.95 us (2%)
    all_gather x1, waiting for transfers between devices, gather_axes(): value = lax.all_gather(value, axis, axis=dim, tiled=True)  68.3 us
    all_to_all x2, blocking collectives, sent_to_all(): lax.all_to_all(jnp.broadcast_to(value[None], (peers, *value.shape)), axis...  47.8 us
    all_gather x1, waiting for transfers between devices, sent_together(): whole, at, outs = (lax.all_gather(both, axis, axis=dim, tiled=True), 0, [])  41 us
    all_to_all x1, blocking collectives, sum_at_owner(): lax.all_to_all(tiles, axis, split_axis=0, concat_axis=0, tiled=True)  34.2 us
    all_to_all x1, waiting for transfers between devices, sum_at_owner(): lax.all_to_all(tiles, axis, split_axis=0, concat_axis=0, tiled=True)  20.6 us
    all_gather x1, blocking collectives, gather_axes(): value = lax.all_gather(value, axis, axis=dim, tiled=True)  16.7 us
    ppermute x3, starting transfers between devices, extended(): before = lax.ppermute(last, axis, up)  12 us
    all_to_all x1, starting transfers between devices, sum_at_owner(): lax.all_to_all(tiles, axis, split_axis=0, concat_axis=0, tiled=True)  9.06 us
  transfers between devices with their start and end apart: 10, of which 5 were waited for; matrix products, arithmetic and copies ran while one was open for 5% of the time, Pallas kernels for 0%

commit v1 on v0

v1 whole, which is shorter than its diff:
```python
import jax
import jax.numpy as jnp
from jax import lax
from jax.experimental import pallas as pl
from jax.experimental.pallas import tpu as pltpu
from jax.sharding import Mesh
from jax.sharding import PartitionSpec as P

HD = 128
WIN = 128
NZ, NY, NX, NC = 16, 4, 4, 2
TOK = 384
D = 2048
FFL = 704
MAIN = 640
TAIL = 64
GU = 2 * FFL
FP = 768
OWN = TOK // (NX * NC)
EPS = 1e-06
LOW = -1e30
COPIES = 140
SP = ("z", "y")
TP = ("x", "c")
F32 = jnp.float32
BF = jnp.bfloat16


def kernel(
    stream,
    query,
    key,
    value,
    doc_col,
    doc_row,
    sink,
    out_w,
    gain,
    gu,
    dn,
    out,
    kext,
    vext,
    dext,
    wg,
    wd,
    ow,
    att,
    carried,
    normed,
    acc,
    hid,
    part,
    summed,
    pair_in,
    opp_in,
    relay,
    near_in,
    far_in,
    send_sems,
    recv_sems,
):
    z, y = lax.axis_index("z"), lax.axis_index("y")
    x, c = lax.axis_index("x"), lax.axis_index("c")
    zr, zl = lax.rem(z + 1, NZ), lax.rem(z + NZ - 1, NZ)
    yr, yl = lax.rem(y + 1, NY), lax.rem(y + NY - 1, NY)
    xr, xl = lax.rem(x + 1, NX), lax.rem(x + NX - 1, NX)
    yo, xo = lax.rem(y + 2, NY), lax.rem(x + 2, NX)
    pc = 1 - c
    sp = z * NY + y
    after, before = lax.rem(sp + 1, NZ * NY), lax.rem(sp + NZ * NY - 1, NZ * NY)
    dev_zr, dev_zl = (zr, y, x, c), (zl, y, x, c)
    dev_yr, dev_yl = (z, yr, x, c), (z, yl, x, c)
    dev_xr, dev_xl = (z, y, xr, c), (z, y, xl, c)
    dev_p = (z, y, x, pc)
    dev_after = (after // NY, lax.rem(after, NY), x, c)
    dev_before = (before // NY, lax.rem(before, NY), x, c)

    barrier = pltpu.get_barrier_semaphore()
    peers = (dev_zr, dev_zl, dev_yr, dev_yl, dev_xr, dev_xl, dev_p, dev_after, dev_before)
    for peer in peers:
        pl.semaphore_signal(barrier, inc=1, device_id=peer, device_id_type=pl.DeviceIdType.MESH)
    pl.semaphore_wait(barrier, len(peers))

    started = []

    def send(src, dst, dev):
        at = len(started)
        copy = pltpu.make_async_remote_copy(
            src_ref=src,
            dst_ref=dst,
            send_sem=send_sems.at[at],
            recv_sem=recv_sems.at[at],
            device_id=dev,
            device_id_type=pl.DeviceIdType.MESH,
        )
        copy.start()
        started.append(copy)
        return copy

    def zm(s):
        return lax.rem(z + NZ - s, NZ)

    def zp(s):
        return lax.rem(z + s, NZ)

    g_zl, g_zr, g_yl, g_yr, g_yo = {}, {}, {}, {}, {}

    def g_to_y(src, at, tag):
        g_yl[tag] = send(src, wg.at[at, y], dev_yr)
        g_yr[tag] = send(src, wg.at[at, y], dev_yl)

    def g_start():
        g_zl[0] = send(gu, wg.at[z, y], dev_zr)
        g_zr[0] = send(gu, wg.at[z, y], dev_zl)
        g_to_y(gu, z, (0, 0))

    def tags(s):
        if s == 0:
            return [(0, 0)]
        if s == 8:
            return [(0, 8)]
        return [(0, s), (1, s)]

    def place(tag):
        return zm(tag[1]) if tag[0] == 0 else zp(tag[1])

    def g_ring(s):
        g_zl[s - 1].wait_recv()
        at = zm(s)
        if s < 8:
            g_zl[s] = send(wg.at[at, y], wg.at[at, y], dev_zr)
        if s <= 7:
            g_zr[s - 1].wait_recv()
            other = zp(s)
            if s < 7:
                g_zr[s] = send(wg.at[other, y], wg.at[other, y], dev_zl)
        for tag in tags(s):
            at = place(tag)
            g_to_y(wg.at[at, y], at, tag)

    def g_across(s):
        for tag in tags(s):
            at = place(tag)
            rightward = (tag[0] == 0 and tag[1] < 8)
            g_yl[tag].wait_recv()
            if rightward:
                g_yo[tag] = send(wg.at[at, yl], wg.at[at, yl], dev_yr)
            g_yr[tag].wait_recv()
            if not rightward:
                g_yo[tag] = send(wg.at[at, yr], wg.at[at, yr], dev_yl)

    def g_done(s):
        for tag in tags(s):
            g_yo[tag].wait_recv()

    d_y, d_zl, d_zr = {}, {}, {}

    def d_start():
        d_y["l"] = send(dn, wd.at[z, y], dev_yr)
        d_y["r"] = send(dn, wd.at[z, y], dev_yl)

    def d_forward():
        d_y["l"].wait_recv()
        d_y["o"] = send(wd.at[z, yl], wd.at[z, yl], dev_yr)
        d_y["r"].wait_recv()

    def d_begin():
        d_y["o"].wait_recv()
        d_zl[0] = send(wd.at[z], wd.at[z], dev_zr)
        d_zr[0] = send(wd.at[z], wd.at[z], dev_zl)

    def d_ring(s):
        d_zl[s - 1].wait_recv()
        if s < 8:
            at = zm(s)
            d_zl[s] = send(wd.at[at], wd.at[at], dev_zr)
        if s <= 7:
            d_zr[s - 1].wait_recv()
            if s < 7:
                other = zp(s)
                d_zr[s] = send(wd.at[other], wd.at[other], dev_zl)

    def x_start(src, slot):
        own = slot(x, c)
        return {"l": send(src, own, dev_xr), "r": send(src, own, dev_xl), "p": send(src, own, dev_p)}

    def x_forward(g, slot, halves):
        left, right = slot(xl, c), slot(xr, c)
        g["l"].wait_recv()
        g["a"] = send(halves(left)[0], halves(left)[0], dev_xr)
        g["pl"] = send(left, left, dev_p)
        g["r"].wait_recv()
        g["b"] = send(halves(right)[1], halves(right)[1], dev_xl)
        g["pr"] = send(right, right, dev_p)

    def x_relay(g, slot, halves):
        a, b = halves(slot(xo, c))
        g["a"].wait_recv()
        g["pa"] = send(a, a, dev_p)
        g["b"].wait_recv()
        g["pb"] = send(b, b, dev_p)

    def x_done(g):
        for name in ("p", "pl", "pr", "pa", "pb"):
            g[name].wait_recv()

    def ow_slot(a, b):
        return ow.at[a * NC + b]

    def ow_halves(ref):
        return ref.at[pl.ds(0, 64)], ref.at[pl.ds(64, 64)]

    def att_slot(a, b):
        return att.at[a * NC + b]

    def att_halves(ref):
        return ref.at[pl.ds(0, 192)], ref.at[pl.ds(192, 192)]

    def out_slot(a, b):
        return out.at[b * NX + a]

    def lane_halves(ref):
        return ref.at[:, pl.ds(0, D // 2)], ref.at[:, pl.ds(D // 2, D // 2)]

    group = pl.multiple_of((x // 2) * HD, HD)
    lanes = pl.ds(group, HD)
    g_start()
    d_start()
    halo = [
        send(key.at[pl.ds(256, 128), lanes], kext.at[pl.ds(0, 128)], dev_after),
        send(value.at[pl.ds(256, 128), lanes], vext.at[pl.ds(0, 128)], dev_after),
        send(doc_row.at[2], dext.at[0], dev_after),
        send(key.at[pl.ds(0, 128), lanes], kext.at[pl.ds(512, 128)], dev_before),
        send(value.at[pl.ds(0, 128), lanes], vext.at[pl.ds(512, 128)], dev_before),
        send(doc_row.at[0], dext.at[1], dev_before),
    ]
    ow_g = x_start(out_w, ow_slot)
    kext[pl.ds(128, 384), :] = key[:, lanes]
    vext[pl.ds(128, 384), :] = value[:, lanes]
    wg[z, y] = gu[...]
    wd[z, y] = dn[...]
    ow[x * NC + c] = out_w[...]
    d_forward()

    for copy in halo:
        copy.wait_recv()
    d_begin()

    def attend(block):
        q = query[pl.ds(block * 128, 128), :]
        k = kext[pl.ds(block * 128, 384), :]
        v = vext[pl.ds(block * 128, 384), :]
        scores = lax.dot_general(q, k, (((1,), (1,)), ((), ())), preferred_element_type=F32)
        scores = scores * HD ** (-0.5)
        if block == 0:
            first = jnp.where(sp == 0, -1, dext[0, 0:1])
        else:
            first = doc_row[block - 1, 0:1]
        if block == 2:
            last = jnp.where(sp == NZ * NY - 1, -1, dext[1, 0:1])
        else:
            last = doc_row[block + 1, 0:1]
        docs = jnp.concatenate([first, doc_row[block, 0:1], last], axis=1)
        mine = doc_col[pl.ds(block * 128, 128), :]
        row = lax.broadcasted_iota(jnp.int32, (128, 384), 0)
        col = lax.broadcasted_iota(jnp.int32, (128, 384), 1)
        allowed = (col >= row) & (col <= row + 2 * WIN) & (mine == docs)
        masked = jnp.where(allowed, scores, LOW)
        here = sink[0]
        peak = jnp.maximum(jnp.max(masked, axis=1, keepdims=True), here)
        lifted = jnp.where(allowed, jnp.exp(masked - peak), 0.0)
        denom = jnp.sum(lifted, axis=1, keepdims=True) + jnp.exp(here - peak)
        probs = (lifted / denom).astype(BF)
        attended = jnp.dot(probs, v, preferred_element_type=F32).astype(BF)
        att[x * NC + c, pl.ds(block * 128, 128), :] = attended

    attend(0)
    g_ring(1)
    attend(1)
    attend(2)
    g_across(0)
    d_ring(1)
    g_ring(2)
    att_g = x_start(att.at[x * NC + c], att_slot)
    g_across(1)
    d_ring(2)
    x_forward(ow_g, ow_slot, ow_halves)
    g_ring(3)
    g_across(2)
    x_forward(att_g, att_slot, att_halves)
    d_ring(3)
    g_ring(4)
    g_across(3)
    x_relay(ow_g, ow_slot, ow_halves)
    x_relay(att_g, att_slot, att_halves)
    d_ring(4)
    x_done(ow_g)
    x_done(att_g)

    def project(n, squares):
        cols = pl.ds(pl.multiple_of(n * 256, 256), 256)
        left = jnp.concatenate([att[h] for h in range(8)], axis=1)
        right = ow[:, :, cols].reshape(1024, 256)
        branch = jnp.dot(left, right, preferred_element_type=F32).astype(BF)
        total = (stream[:, cols].astype(F32) + branch.astype(F32)).astype(BF)
        carried[:, :, cols] = total.reshape(8, OWN, 256)
        wide = total.astype(F32)
        return squares + jnp.sum(wide * wide, axis=1, keepdims=True)

    squares = lax.fori_loop(0, 8, project, jnp.zeros((TOK, 1), F32))
    scale = lax.rsqrt(squares / D + EPS)

    g_ring(5)

    def normalize(n, carry):
        cols = pl.ds(pl.multiple_of(n * 256, 256), 256)
        wide = carried[:, :, cols].reshape(TOK, 256).astype(F32)
        normed[:, cols] = (wide * scale * gain[:, cols]).astype(BF)
        return carry

    lax.fori_loop(0, 8, normalize, 0)
    g_across(4)
    d_ring(5)
    g_ring(6)

    def accumulate(za, zb, first):
        left = jnp.concatenate(
            [
                normed[:, pl.ds(pl.multiple_of(za * 128, 128), 128)],
                normed[:, pl.ds(pl.multiple_of(zb * 128, 128), 128)],
            ],
            axis=1,
        )
        for lo, size in ((0, 512), (512, 512), (1024, 384)):
            cols = pl.ds(lo, size)
            right = jnp.concatenate(
                [wg[za, :, :, cols].reshape(128, size), wg[zb, :, :, cols].reshape(128, size)], axis=0
            )
            term = jnp.dot(left, right, preferred_element_type=F32)
            if first:
                acc[:, cols] = term
            else:
                acc[:, cols] += term

    def accumulate_tag(s, first=False):
        accumulate(zm(s), zp(s), first)

    g_done(1)
    accumulate_tag(1, True)
    g_across(5)
    d_ring(6)
    g_done(2)
    g_done(3)

    def both(i, carry):
        accumulate_tag(i)
        return carry

    lax.fori_loop(2, 4, both, 0)
    g_ring(7)
    g_across(6)
    d_ring(7)
    g_done(4)
    accumulate_tag(4)
    g_ring(8)
    g_across(7)
    d_ring(8)
    g_done(5)
    accumulate_tag(5)
    g_across(8)
    g_done(6)
    accumulate_tag(6)
    g_done(7)
    accumulate_tag(7)
    g_done(0)
    g_done(8)
    accumulate(z, zm(8), False)

    gate, up = acc[:, 0:MAIN], acc[:, MAIN : 2 * MAIN]
    hid[:, 0:MAIN] = (gate / (1.0 + jnp.exp(-gate)) * up).astype(BF)
    rest = acc[:, 2 * MAIN : GU]
    swapped = pltpu.roll(rest, TAIL, 1)
    tail = (rest / (1.0 + jnp.exp(-rest)) * swapped).astype(BF)
    lane = lax.broadcasted_iota(jnp.int32, (TOK, 2 * TAIL), 1)
    hid[:, MAIN:FP] = jnp.where(lane < TAIL, tail.astype(F32), 0.0).astype(BF)

    def lower(n, carry):
        w = wd[pl.ds(2 * n, 2)].reshape(256, FP)
        term = lax.dot_general(hid[...], w, (((1,), (1,)), ((), ())), preferred_element_type=F32)
        cols = pl.ds(pl.multiple_of(n * 256, 256), 256)
        part[:, :, :, cols] = term.astype(BF).reshape(NC, NX, OWN, 256)
        return carry

    lax.fori_loop(0, 8, lower, 0)

    to_pair = send(part.at[pc], pair_in, dev_p)
    to_pair.wait_recv()

    def fold(i, carry):
        at = lax.rem(xo + i, NX)
        summed[at] = (part[c, at].astype(F32) + pair_in[at].astype(F32)).astype(BF)
        return carry

    lax.fori_loop(0, 4, fold, 0)
    half = D // 2
    low, high = pl.ds(0, half), pl.ds(half, half)
    opp_a = send(summed.at[xo, :, low], opp_in.at[0], dev_xr)
    opp_b = send(summed.at[xo, :, high], opp_in.at[1], dev_xl)
    near_b = send(summed.at[xr, :, high], near_in.at[1], dev_xr)
    near_a = send(summed.at[xl, :, low], near_in.at[0], dev_xl)
    opp_a.wait_recv()
    relay[0] = (opp_in[0].astype(F32) + summed[xr, :, low].astype(F32)).astype(BF)
    opp_b.wait_recv()
    relay[1] = (opp_in[1].astype(F32) + summed[xl, :, high].astype(F32)).astype(BF)
    far_a = send(relay.at[0], far_in.at[0], dev_xr)
    far_b = send(relay.at[1], far_in.at[1], dev_xl)
    near_a.wait_recv()
    near_b.wait_recv()
    own = c * NX + x
    for i, arrived in ((0, far_a), (1, far_b)):
        arrived.wait_recv()
        cols = pl.ds(i * half, half)
        feed = summed[x, :, cols].astype(F32) + near_in[i].astype(F32) + far_in[i].astype(F32)
        feed = feed.astype(BF).astype(F32)
        out[own, :, cols] = (carried[own, :, cols].astype(F32) + 0.5 * feed).astype(BF)
    out_g = x_start(out.at[own], out_slot)
    x_forward(out_g, out_slot, lane_halves)
    x_relay(out_g, out_slot, lane_halves)
    x_done(out_g)
    for copy in started:
        copy.wait_send()


def per_device(
    stream,
    query_rows,
    key_rows,
    value_rows,
    doc_ids,
    sink_logit,
    out_weight,
    norm_gain,
    gate_weight,
    up_weight,
    down_weight,
):
    gu = jnp.concatenate(
        [gate_weight[:, :MAIN], up_weight[:, :MAIN], gate_weight[:, MAIN:], up_weight[:, MAIN:]], axis=1
    )
    dn = jnp.pad(down_weight.T, ((0, 0), (0, FP - FFL)))
    doc_col = doc_ids.reshape(TOK, 1)
    doc_row = jnp.broadcast_to(doc_ids.reshape(3, 1, 128), (3, 8, 128))
    vmem = pl.BlockSpec(memory_space=pltpu.VMEM)
    smem = pl.BlockSpec(memory_space=pltpu.SMEM)
    result = pl.pallas_call(
        kernel,
        out_shape=jax.ShapeDtypeStruct((8, OWN, D), BF),
        in_specs=[vmem] * 6 + [smem] + [vmem] * 4,
        out_specs=vmem,
        scratch_shapes=[
            pltpu.VMEM((TOK + 2 * WIN, HD), BF),
            pltpu.VMEM((TOK + 2 * WIN, HD), BF),
            pltpu.VMEM((2, 8, 128), jnp.int32),
            pltpu.VMEM((NZ, NY, 32, GU), BF),
            pltpu.VMEM((NZ, NY, 32, FP), BF),
            pltpu.VMEM((8, 128, D), BF),
            pltpu.VMEM((8, TOK, HD), BF),
            pltpu.VMEM((8, OWN, D), BF),
            pltpu.VMEM((TOK, D), BF),
            pltpu.VMEM((TOK, GU), F32),
            pltpu.VMEM((TOK, FP), BF),
            pltpu.VMEM((NC, NX, OWN, D), BF),
            pltpu.VMEM((NX, OWN, D), BF),
            pltpu.VMEM((NX, OWN, D), BF),
            pltpu.VMEM((2, OWN, D // 2), BF),
            pltpu.VMEM((2, OWN, D // 2), BF),
            pltpu.VMEM((2, OWN, D // 2), BF),
            pltpu.VMEM((2, OWN, D // 2), BF),
            pltpu.SemaphoreType.DMA((COPIES,)),
            pltpu.SemaphoreType.DMA((COPIES,)),
        ],
        compiler_params=pltpu.CompilerParams(
            collective_id=0, has_side_effects=True, vmem_limit_bytes=60 * 1024 * 1024
        ),
    )(
        stream,
        query_rows,
        key_rows,
        value_rows,
        doc_col,
        doc_row,
        sink_logit,
        out_weight,
        norm_gain.reshape(1, D),
        gu,
        dn,
    )
    return result.reshape(TOK, D)


def solution(mesh):
    split = Mesh(mesh.devices.reshape(NZ, NY, NX, NC), ("z", "y", "x", "c"))
    placed = (
        P(SP, None),
        P(SP, TP),
        P(SP, None),
        P(SP, None),
        P(SP),
        P(TP),
        P(TP, None),
        P(),
        P(SP, TP),
        P(SP, TP),
        P(TP, SP),
    )
    return jax.shard_map(
        per_device, mesh=split, in_specs=placed, out_specs=P(SP, None), check_vma=False
    )
```

time: 309 us -> 121 us (0.39)
  waiting for transfers between devices: 134 us -> 0 us
  Pallas kernels: 0 us -> 109 us
  blocking collectives: 98.6 us -> 0 us
  starting transfers between devices: 29.1 us -> 0 us
  matrix products: 14.7 us -> 0 us
  between operations: 14.3 us -> 0.66 us
  other arithmetic: 4.95 us -> 0 us
    all_gather x2 -> x0, waiting for transfers between devices: 109 us -> none  [the longest x1 68.3 us: gather_axes(): value = lax.all_gather(value, axis, axis=dim, tiled=True)]
    pallas_call x0 -> x1, Pallas kernels: none -> 109 us  [per_device(): pl.pallas_call(kernel, out_shape=jax.ShapeDtypeStruct((8, OWN, D), BF), i...]
    all_to_all x3 -> x0, blocking collectives: 81.9 us -> none  [the longest x2 47.8 us: sent_to_all(): lax.all_to_all(jnp.broadcast_to(value[None], (peers, *value.shape)), axis...]
    all_to_all x2 -> x0, waiting for transfers between devices: 24.5 us -> none  [the longest x1 20.6 us: sum_at_owner(): lax.all_to_all(tiles, axis, split_axis=0, concat_axis=0, tiled=True)]
    all_gather x1 -> x0, blocking collectives: 16.7 us -> none  [gather_axes(): value = lax.all_gather(value, axis, axis=dim, tiled=True)]
    ppermute x6 -> x0, starting transfers between devices: 15.8 us -> none  [the longest x3 12 us: extended(): before = lax.ppermute(last, axis, up)]
    dot_general x4 -> x0, matrix products: 14.7 us -> none  [the longest x1 8.21 us: per_device(): jnp.dot(hidden, gather_axes(down_weight, SP, 1), preferred_element_type=j...]
    all_to_all x2 -> x0, starting transfers between devices: 13.3 us -> none  [the longest x1 9.06 us: sum_at_owner(): lax.all_to_all(tiles, axis, split_axis=0, concat_axis=0, tiled=True)]
  transfers between devices with their start and end apart: 10 -> 0, of which waited for: 5 -> 0; matrix products, arithmetic and copies ran while one was open for 5% -> 0% of each run, Pallas kernels for 0% -> 0%
where the time goes in v1:
time: 121 us; the launch traced here: 120 us
  Pallas kernels  109 us (90%)
  local copies, waits for them, and re-layouts  10.6 us (9%)
    pallas_call x1, Pallas kernels, per_device(): pl.pallas_call(kernel, out_shape=jax.ShapeDtypeStruct((8, OWN, D), BF), i...  109 us
    unnamed x1, local copies, waits for them, and re-layouts  2.73 us

profile of v1, /device:TPU:1, one launch (start us, length us, event | category | flops | bytes accessed | tf_op | source)
XLA Modules:
  0.0 120.1 jit_solution(11679091823699256114)
XLA Ops:
  0.7 0.7 slice.14
  1.4 0.7 slice.15
  2.1 1.3 %broadcast_in_dim.8.doc_row = s32[3,8,128]{2,1,0:T(8,128)} broadcast(s32[3,128]{1,0:T(4,128)} %bitcast.7), dimensions={0,2} | broadcast | bytes 13824 | tf_op jit(solution)/shard_map/broadcast_in_dim | solution.py:453
  3.3 0.8 slice.12
  4.1 0.8 slice.13
  4.9 0.7 concatenate.3.gu
  5.6 1.4 %pad.4.dn = bf16[32,768]{1,0:T(8,128)(2,1)} pad(bf16[32,704]{1,0:T(8,128)(2,1)} %bitcast.5, bf16[]{:T(256)} %constant.2.clone.1), padding=0_0x0_64 | pad | bytes 94210 | tf_op jit(solution)/shard_map/jit(_pad)/pad | solution.py:451
  7.0 1.5 %reshape.14.doc_col = s32[384,1]{1,0:T(8,128)} reshape(s32[384]{0:T(512)} %param.15) | data formatting | bytes 3072 | tf_op jit(solution)/shard_map/reshape | solution.py:452
  8.5 108.9 %shard_map.109 = bf16[8,48,2048]{2,1,0:T(8,128)(2,1)} custom-call(bf16[384,2048]{1,0:T(8,128)(2,1)} %stream.1, bf16[384,128]{1,0:T(8,128)(2,1)} %query.1, bf16[384,256]{1,0:T(8,128)(2,1)} %key.1, bf16[384,256]{1,0:T(8,128)(2,1)} %value.1, s32[384,1]{1,0:T(8,128)} %reshape.14.doc_col, s32[3,8,128]{2,1,0:T(8,128)} %broadcast_in_dim.8.doc_row, ...), custom_call_target="tpu_custom_call" | custom-call | tf_op jit(solution)/shard_map/pallas_call | solution.py:456
  117.4 2.7 %copy.15 = bf16[384,2048]{1,0:T(8,128)(2,1)} copy(bf16[384,2048]{1,0:T(8,128)(2,1)} %bitcast.4) | data formatting | bytes 3145728

commit v2 on v1

--- a/solution.py
+++ b/solution.py
@@ -14,12 +14,11 @@
 FFL = 704
 MAIN = 640
 TAIL = 64
-GU = 2 * FFL
 FP = 768
 OWN = TOK // (NX * NC)
 EPS = 1e-06
 LOW = -1e30
-COPIES = 140
+COPIES = 260
 SP = ("z", "y")
 TP = ("x", "c")
 F32 = jnp.float32
@@ -27,28 +26,34 @@
 
 
 def kernel(
-    stream,
+    stream_far,
     query,
     key,
     value,
-    doc_col,
-    doc_row,
+    docs,
     sink,
     out_w,
     gain,
-    gu,
-    dn,
+    gate_w,
+    up_w,
+    down_w,
     out,
+    stream,
     kext,
     vext,
+    dsend,
     dext,
-    wg,
+    gb_own,
+    dn_own,
+    wga,
+    wgb,
     wd,
     ow,
     att,
     carried,
     normed,
-    acc,
+    acc_a,
+    acc_b,
     hid,
     part,
     summed,
@@ -57,6 +62,7 @@
     relay,
     near_in,
     far_in,
+    local_sem,
     send_sems,
     recv_sems,
 ):
@@ -80,6 +86,23 @@
     peers = (dev_zr, dev_zl, dev_yr, dev_yl, dev_xr, dev_xl, dev_p, dev_after, dev_before)
     for peer in peers:
         pl.semaphore_signal(barrier, inc=1, device_id=peer, device_id_type=pl.DeviceIdType.MESH)
+    stream_copy = pltpu.make_async_copy(stream_far, stream, local_sem)
+    stream_copy.start()
+
+    gb_own[:, 0:MAIN] = up_w[:, 0:MAIN]
+    gb_own[:, MAIN:FP] = jnp.concatenate([gate_w[:, MAIN:FFL], up_w[:, MAIN:FFL]], axis=1)
+    dn_own[:, 0:MAIN] = down_w[:, 0:MAIN]
+    dn_own[:, MAIN:FP] = jnp.concatenate([down_w[:, MAIN:FFL], jnp.zeros((32, TAIL), BF)], axis=1)
+    dsend[0] = jnp.broadcast_to(docs[2:3], (8, 128))
+    dsend[1] = jnp.broadcast_to(docs[0:1], (8, 128))
+    group = pl.multiple_of((x // 2) * HD, HD)
+    lanes = pl.ds(group, HD)
+    kext[pl.ds(128, 384), :] = key[:, lanes]
+    vext[pl.ds(128, 384), :] = value[:, lanes]
+    wga[z, y] = gate_w[:, 0:MAIN]
+    wgb[z, y] = gb_own[...]
+    wd[z, y] = dn_own[...]
+
     pl.semaphore_wait(barrier, len(peers))
 
     started = []
@@ -104,17 +127,6 @@
     def zp(s):
         return lax.rem(z + s, NZ)
 
-    g_zl, g_zr, g_yl, g_yr, g_yo = {}, {}, {}, {}, {}
-
-    def g_to_y(src, at, tag):
-        g_yl[tag] = send(src, wg.at[at, y], dev_yr)
-        g_yr[tag] = send(src, wg.at[at, y], dev_yl)
-
-    def g_start():
-        g_zl[0] = send(gu, wg.at[z, y], dev_zr)
-        g_zr[0] = send(gu, wg.at[z, y], dev_zl)
-        g_to_y(gu, z, (0, 0))
-
     def tags(s):
         if s == 0:
             return [(0, 0)]
@@ -125,61 +137,86 @@
     def place(tag):
         return zm(tag[1]) if tag[0] == 0 else zp(tag[1])
 
-    def g_ring(s):
-        g_zl[s - 1].wait_recv()
-        at = zm(s)
-        if s < 8:
-            g_zl[s] = send(wg.at[at, y], wg.at[at, y], dev_zr)
-        if s <= 7:
-            g_zr[s - 1].wait_recv()
-            other = zp(s)
-            if s < 7:
-                g_zr[s] = send(wg.at[other, y], wg.at[other, y], dev_zl)
-        for tag in tags(s):
-            at = place(tag)
-            g_to_y(wg.at[at, y], at, tag)
-
-    def g_across(s):
-        for tag in tags(s):
-            at = place(tag)
-            rightward = (tag[0] == 0 and tag[1] < 8)
-            g_yl[tag].wait_recv()
-            if rightward:
-                g_yo[tag] = send(wg.at[at, yl], wg.at[at, yl], dev_yr)
-            g_yr[tag].wait_recv()
-            if not rightward:
-                g_yo[tag] = send(wg.at[at, yr], wg.at[at, yr], dev_yl)
-
-    def g_done(s):
-        for tag in tags(s):
-            g_yo[tag].wait_recv()
-
-    d_y, d_zl, d_zr = {}, {}, {}
-
-    def d_start():
-        d_y["l"] = send(dn, wd.at[z, y], dev_yr)
-        d_y["r"] = send(dn, wd.at[z, y], dev_yl)
-
-    def d_forward():
-        d_y["l"].wait_recv()
-        d_y["o"] = send(wd.at[z, yl], wd.at[z, yl], dev_yr)
-        d_y["r"].wait_recv()
-
-    def d_begin():
-        d_y["o"].wait_recv()
-        d_zl[0] = send(wd.at[z], wd.at[z], dev_zr)
-        d_zr[0] = send(wd.at[z], wd.at[z], dev_zl)
-
-    def d_ring(s):
-        d_zl[s - 1].wait_recv()
-        if s < 8:
-            at = zm(s)
-            d_zl[s] = send(wd.at[at], wd.at[at], dev_zr)
-        if s <= 7:
-            d_zr[s - 1].wait_recv()
-            if s < 7:
-                other = zp(s)
-                d_zr[s] = send(wd.at[other], wd.at[other], dev_zl)
+    class ZFirst:
+        def __init__(self, own, buf):
+            self.own, self.buf = own, buf
+            self.left, self.right, self.yl, self.yr, self.yo = {}, {}, {}, {}, {}
+
+        def to_y(self, src, at, tag):
+            self.yl[tag] = send(src, self.buf.at[at, y], dev_yr)
+            self.yr[tag] = send(src, self.buf.at[at, y], dev_yl)
+
+        def start(self):
+            self.left[0] = send(self.own, self.buf.at[z, y], dev_zr)
+            self.right[0] = send(self.own, self.buf.at[z, y], dev_zl)
+            self.to_y(self.own, z, (0, 0))
+
+        def ring(self, s):
+            block = self.buf.at[zm(s), y]
+            self.left[s - 1].wait_recv()
+            if s < 8:
+                self.left[s] = send(block, block, dev_zr)
+            if s <= 7:
+                block = self.buf.at[zp(s), y]
+                self.right[s - 1].wait_recv()
+                if s < 7:
+                    self.right[s] = send(block, block, dev_zl)
+            for tag in tags(s):
+                at = place(tag)
+                self.to_y(self.buf.at[at, y], at, tag)
+
+        def across(self, s):
+            for tag in tags(s):
+                at = place(tag)
+                rightward = tag[0] == 0 and tag[1] < 8
+                self.yl[tag].wait_recv()
+                if rightward:
+                    self.yo[tag] = send(self.buf.at[at, yl], self.buf.at[at, yl], dev_yr)
+                self.yr[tag].wait_recv()
+                if not rightward:
+                    self.yo[tag] = send(self.buf.at[at, yr], self.buf.at[at, yr], dev_yl)
+
+        def done(self, s):
+            for tag in tags(s):
+                self.yo[tag].wait_recv()
+
+    class YFirst:
+        def __init__(self, own, buf):
+            self.own, self.buf = own, buf
+            self.left, self.right = {}, {}
+
+        def begin_piece(self, p, col, src):
+            self.left[p, 0] = send(src, self.buf.at[z, col], dev_zr)
+            self.right[p, 0] = send(src, self.buf.at[z, col], dev_zl)
+
+        def start(self):
+            self.from_l = send(self.own, self.buf.at[z, y], dev_yr)
+            self.from_r = send(self.own, self.buf.at[z, y], dev_yl)
+            self.begin_piece(0, y, self.own)
+
+        def begin(self):
+            self.from_l.wait_recv()
+            block = self.buf.at[z, yl]
+            self.from_o = send(block, block, dev_yr)
+            self.begin_piece(1, yl, block)
+            self.from_r.wait_recv()
+            self.begin_piece(2, yr, self.buf.at[z, yr])
+
+        def begin_last(self):
+            self.from_o.wait_recv()
+            self.begin_piece(3, yo, self.buf.at[z, yo])
+
+        def ring(self, s):
+            for p, col in enumerate((y, yl, yr, yo)):
+                self.left[p, s - 1].wait_recv()
+                if s < 8:
+                    block = self.buf.at[zm(s), col]
+                    self.left[p, s] = send(block, block, dev_zr)
+                if s <= 7:
+                    self.right[p, s - 1].wait_recv()
+                    if s < 7:
+                        block = self.buf.at[zp(s), col]
+                        self.right[p, s] = send(block, block, dev_zl)
 
     def x_start(src, slot):
         own = slot(x, c)
@@ -223,29 +260,22 @@
     def lane_halves(ref):
         return ref.at[:, pl.ds(0, D // 2)], ref.at[:, pl.ds(D // 2, D // 2)]
 
-    group = pl.multiple_of((x // 2) * HD, HD)
-    lanes = pl.ds(group, HD)
-    g_start()
-    d_start()
+    ga = ZFirst(gate_w.at[:, pl.ds(0, MAIN)], wga)
+    gb = YFirst(gb_own, wgb)
+    dn = ZFirst(dn_own, wd)
     halo = [
         send(key.at[pl.ds(256, 128), lanes], kext.at[pl.ds(0, 128)], dev_after),
         send(value.at[pl.ds(256, 128), lanes], vext.at[pl.ds(0, 128)], dev_after),
-        send(doc_row.at[2], dext.at[0], dev_after),
+        send(dsend.at[0], dext.at[0], dev_after),
         send(key.at[pl.ds(0, 128), lanes], kext.at[pl.ds(512, 128)], dev_before),
         send(value.at[pl.ds(0, 128), lanes], vext.at[pl.ds(512, 128)], dev_before),
-        send(doc_row.at[0], dext.at[1], dev_before),
+        send(dsend.at[1], dext.at[1], dev_before),
     ]
+    gb.start()
+    ga.start()
     ow_g = x_start(out_w, ow_slot)
-    kext[pl.ds(128, 384), :] = key[:, lanes]
-    vext[pl.ds(128, 384), :] = value[:, lanes]
-    wg[z, y] = gu[...]
-    wd[z, y] = dn[...]
     ow[x * NC + c] = out_w[...]
-    d_forward()
-
-    for copy in halo:
-        copy.wait_recv()
-    d_begin()
+    gb.begin()
 
     def attend(block):
         q = query[pl.ds(block * 128, 128), :]
@@ -256,16 +286,16 @@
         if block == 0:
             first = jnp.where(sp == 0, -1, dext[0, 0:1])
         else:
-            first = doc_row[block - 1, 0:1]
+            first = docs[block - 1 : block]
         if block == 2:
             last = jnp.where(sp == NZ * NY - 1, -1, dext[1, 0:1])
         else:
-            last = doc_row[block + 1, 0:1]
-        docs = jnp.concatenate([first, doc_row[block, 0:1], last], axis=1)
-        mine = doc_col[pl.ds(block * 128, 128), :]
+            last = docs[block + 1 : block + 2]
+        around = jnp.concatenate([first, docs[block : block + 1], last], axis=1)
+        mine = jnp.transpose(jnp.broadcast_to(docs[block : block + 1], (128, 128)))[:, 0:1]
         row = lax.broadcasted_iota(jnp.int32, (128, 384), 0)
         col = lax.broadcasted_iota(jnp.int32, (128, 384), 1)
-        allowed = (col >= row) & (col <= row + 2 * WIN) & (mine == docs)
+        allowed = (col >= row) & (col <= row + 2 * WIN) & (mine == around)
         masked = jnp.where(allowed, scores, LOW)
         here = sink[0]
         peak = jnp.maximum(jnp.max(masked, axis=1, keepdims=True), here)
@@ -275,28 +305,36 @@
         attended = jnp.dot(probs, v, preferred_element_type=F32).astype(BF)
         att[x * NC + c, pl.ds(block * 128, 128), :] = attended
 
+    attend(1)
+    gb.begin_last()
+    for copy in halo:
+        copy.wait_recv()
     attend(0)
-    g_ring(1)
-    attend(1)
+    ga.ring(1)
+    gb.ring(1)
     attend(2)
-    g_across(0)
-    d_ring(1)
-    g_ring(2)
+    ga.across(0)
+    ga.ring(2)
+    gb.ring(2)
     att_g = x_start(att.at[x * NC + c], att_slot)
-    g_across(1)
-    d_ring(2)
+    ga.across(1)
+    dn.start()
     x_forward(ow_g, ow_slot, ow_halves)
-    g_ring(3)
-    g_across(2)
+    ga.ring(3)
+    gb.ring(3)
     x_forward(att_g, att_slot, att_halves)
-    d_ring(3)
-    g_ring(4)
-    g_across(3)
+    ga.across(2)
+    dn.ring(1)
+    ga.ring(4)
+    gb.ring(4)
     x_relay(ow_g, ow_slot, ow_halves)
     x_relay(att_g, att_slot, att_halves)
-    d_ring(4)
+    ga.across(3)
+    dn.across(0)
+    dn.ring(2)
     x_done(ow_g)
     x_done(att_g)
+    stream_copy.wait()
 
     def project(n, squares):
         cols = pl.ds(pl.multiple_of(n * 256, 256), 256)
@@ -311,7 +349,8 @@
     squares = lax.fori_loop(0, 8, project, jnp.zeros((TOK, 1), F32))
     scale = lax.rsqrt(squares / D + EPS)
 
-    g_ring(5)
+    ga.ring(5)
+    gb.ring(5)
 
     def normalize(n, carry):
         cols = pl.ds(pl.multiple_of(n * 256, 256), 256)
@@ -320,9 +359,9 @@
         return carry
 
     lax.fori_loop(0, 8, normalize, 0)
-    g_across(4)
-    d_ring(5)
-    g_ring(6)
+    ga.across(4)
+    dn.across(1)
+    dn.ring(3)
 
     def accumulate(za, zb, first):
         left = jnp.concatenate(
@@ -332,58 +371,70 @@
             ],
             axis=1,
         )
-        for lo, size in ((0, 512), (512, 512), (1024, 384)):
-            cols = pl.ds(lo, size)
-            right = jnp.concatenate(
-                [wg[za, :, :, cols].reshape(128, size), wg[zb, :, :, cols].reshape(128, size)], axis=0
-            )
+        for buf, acc, width in ((wga, acc_a, MAIN), (wgb, acc_b, FP)):
+            right = jnp.concatenate([buf[za].reshape(128, width), buf[zb].reshape(128, width)], axis=0)
             term = jnp.dot(left, right, preferred_element_type=F32)
             if first:
-                acc[:, cols] = term
+                acc[...] = term
             else:
-                acc[:, cols] += term
+                acc[...] += term
 
     def accumulate_tag(s, first=False):
         accumulate(zm(s), zp(s), first)
 
-    g_done(1)
+    ga.done(1)
     accumulate_tag(1, True)
-    g_across(5)
-    d_ring(6)
-    g_done(2)
-    g_done(3)
+    ga.ring(6)
+    gb.ring(6)
+    ga.across(5)
+    dn.across(2)
+    dn.ring(4)
+    ga.done(2)
+    ga.done(3)
 
     def both(i, carry):
         accumulate_tag(i)
         return carry
 
     lax.fori_loop(2, 4, both, 0)
-    g_ring(7)
-    g_across(6)
-    d_ring(7)
-    g_done(4)
+    ga.ring(7)
+    gb.ring(7)
+    ga.across(6)
+    dn.across(3)
+    dn.ring(5)
+    ga.done(4)
     accumulate_tag(4)
-    g_ring(8)
-    g_across(7)
-    d_ring(8)
-    g_done(5)
+    ga.ring(8)
+    gb.ring(8)
+    ga.across(7)
+    dn.across(4)
+    dn.ring(6)
+    ga.done(5)
     accumulate_tag(5)
-    g_across(8)
-    g_done(6)
+    ga.across(8)
+    dn.across(5)
+    dn.ring(7)
+    ga.done(6)
     accumulate_tag(6)
-    g_done(7)
+    ga.done(7)
     accumulate_tag(7)
-    g_done(0)
-    g_done(8)
+    dn.across(6)
+    dn.ring(8)
+    ga.done(0)
+    ga.done(8)
     accumulate(z, zm(8), False)
-
-    gate, up = acc[:, 0:MAIN], acc[:, MAIN : 2 * MAIN]
+    dn.across(7)
+
+    gate, up = acc_a[...], acc_b[:, 0:MAIN]
     hid[:, 0:MAIN] = (gate / (1.0 + jnp.exp(-gate)) * up).astype(BF)
-    rest = acc[:, 2 * MAIN : GU]
+    rest = acc_b[:, MAIN:FP]
     swapped = pltpu.roll(rest, TAIL, 1)
-    tail = (rest / (1.0 + jnp.exp(-rest)) * swapped).astype(BF)
+    tail = rest / (1.0 + jnp.exp(-rest)) * swapped
     lane = lax.broadcasted_iota(jnp.int32, (TOK, 2 * TAIL), 1)
-    hid[:, MAIN:FP] = jnp.where(lane < TAIL, tail.astype(F32), 0.0).astype(BF)
+    hid[:, MAIN:FP] = jnp.where(lane < TAIL, tail, 0.0).astype(BF)
+    dn.across(8)
+    for s in range(9):
+        dn.done(s)
 
     def lower(n, carry):
         w = wd[pl.ds(2 * n, 2)].reshape(256, FP)
@@ -445,30 +496,32 @@
     up_weight,
     down_weight,
 ):
-    gu = jnp.concatenate(
-        [gate_weight[:, :MAIN], up_weight[:, :MAIN], gate_weight[:, MAIN:], up_weight[:, MAIN:]], axis=1
-    )
-    dn = jnp.pad(down_weight.T, ((0, 0), (0, FP - FFL)))
-    doc_col = doc_ids.reshape(TOK, 1)
-    doc_row = jnp.broadcast_to(doc_ids.reshape(3, 1, 128), (3, 8, 128))
     vmem = pl.BlockSpec(memory_space=pltpu.VMEM)
     smem = pl.BlockSpec(memory_space=pltpu.SMEM)
+    far = pl.BlockSpec(memory_space=pl.ANY)
     result = pl.pallas_call(
         kernel,
+        name="layer",
         out_shape=jax.ShapeDtypeStruct((8, OWN, D), BF),
-        in_specs=[vmem] * 6 + [smem] + [vmem] * 4,
+        in_specs=[far] + [vmem] * 4 + [smem] + [vmem] * 5,
         out_specs=vmem,
         scratch_shapes=[
+            pltpu.VMEM((TOK, D), BF),
             pltpu.VMEM((TOK + 2 * WIN, HD), BF),
             pltpu.VMEM((TOK + 2 * WIN, HD), BF),
             pltpu.VMEM((2, 8, 128), jnp.int32),
-            pltpu.VMEM((NZ, NY, 32, GU), BF),
+            pltpu.VMEM((2, 8, 128), jnp.int32),
+            pltpu.VMEM((32, FP), BF),
+            pltpu.VMEM((32, FP), BF),
+            pltpu.VMEM((NZ, NY, 32, MAIN), BF),
+            pltpu.VMEM((NZ, NY, 32, FP), BF),
             pltpu.VMEM((NZ, NY, 32, FP), BF),
             pltpu.VMEM((8, 128, D), BF),
             pltpu.VMEM((8, TOK, HD), BF),
             pltpu.VMEM((8, OWN, D), BF),
             pltpu.VMEM((TOK, D), BF),
-            pltpu.VMEM((TOK, GU), F32),
+            pltpu.VMEM((TOK, MAIN), F32),
+            pltpu.VMEM((TOK, FP), F32),
             pltpu.VMEM((TOK, FP), BF),
             pltpu.VMEM((NC, NX, OWN, D), BF),
             pltpu.VMEM((NX, OWN, D), BF),
@@ -477,6 +530,7 @@
             pltpu.VMEM((2, OWN, D // 2), BF),
             pltpu.VMEM((2, OWN, D // 2), BF),
             pltpu.VMEM((2, OWN, D // 2), BF),
+            pltpu.SemaphoreType.DMA,
             pltpu.SemaphoreType.DMA((COPIES,)),
             pltpu.SemaphoreType.DMA((COPIES,)),
         ],
@@ -488,13 +542,13 @@
         query_rows,
         key_rows,
         value_rows,
-        doc_col,
-        doc_row,
+        doc_ids.reshape(3, 128),
         sink_logit,
         out_weight,
         norm_gain.reshape(1, D),
-        gu,
-        dn,
+        gate_weight,
+        up_weight,
+        down_weight.T,
     )
     return result.reshape(TOK, D)
 

time: 121 us -> 119 us (0.983)
  local copies, waits for them, and re-layouts: 10.6 us -> 2.73 us
  Pallas kernels: 109 us -> 115 us
    pallas_call x1, Pallas kernels: 109 us -> 115 us  [per_device(): pl.pallas_call(kernel, name='layer', out_shape=jax.ShapeDtypeStruct((8, O...]
    slice x4 -> x0, local copies, waits for them, and re-layouts: 2.96 us -> none  [the longest x1 0.78 us: per_device(): gate_weight[:, :MAIN]]
    reshape x1 -> x0, local copies, waits for them, and re-layouts: 1.47 us -> none  [per_device(): doc_col = doc_ids.reshape(TOK, 1)]
    pad x1 -> x0, local copies, waits for them, and re-layouts: 1.42 us -> none  [per_device(): dn = jnp.pad(down_weight.T, ((0, 0), (0, FP - FFL)))]
    broadcast_in_dim x1 -> x0, local copies, waits for them, and re-layouts: 1.28 us -> none  [per_device(): doc_row = jnp.broadcast_to(doc_ids.reshape(3, 1, 128), (3, 8, 128))]
where the time goes in v2:
time: 119 us
  Pallas kernels  115 us (97%)
  local copies, waits for them, and re-layouts  2.73 us (2%)
    pallas_call x1, Pallas kernels, per_device(): pl.pallas_call(kernel, name='layer', out_shape=jax.ShapeDtypeStruct((8, O...  115 us
    unnamed x1, local copies, waits for them, and re-layouts  2.73 us

profile of v2, /device:TPU:1, one launch (start us, length us, event | category | flops | bytes accessed | tf_op | source)
XLA Modules:
  0.0 118.5 jit_solution(17919525431878530839)
XLA Ops:
  0.7 115.1 %layer.1 = bf16[8,48,2048]{2,1,0:T(8,128)(2,1)} custom-call(bf16[384,2048]{1,0:T(8,128)(2,1)} %stream_far.1, bf16[384,128]{1,0:T(8,128)(2,1)} %query.1, bf16[384,256]{1,0:T(8,128)(2,1)} %key.1, bf16[384,256]{1,0:T(8,128)(2,1)} %value.1, s32[3,128]{1,0:T(4,128)} %bitcast.7, f32[1]{0:T(128)S(6)} %copy.13.sink, bf16[128,2048]{1,0:T(8,128)(2,1)} %out_w.1, ...), custom_call_target="tpu_custom_call" | custom-call | tf_op jit(solution)/shard_map/layer/pallas_call | solution.py:502
  115.8 2.7 %copy.14 = bf16[384,2048]{1,0:T(8,128)(2,1)} copy(bf16[384,2048]{1,0:T(8,128)(2,1)} %bitcast.4) | data formatting | bytes 3145728

commit v3 on v2

--- a/solution.py
+++ b/solution.py
@@ -18,7 +18,9 @@
 OWN = TOK // (NX * NC)
 EPS = 1e-06
 LOW = -1e30
-COPIES = 260
+COPIES = 280
+CHUNK = D // 4
+HALF = CHUNK // 2
 SP = ("z", "y")
 TP = ("x", "c")
 F32 = jnp.float32
@@ -62,7 +64,9 @@
     relay,
     near_in,
     far_in,
+    shuffled,
     local_sem,
+    out_sems,
     send_sems,
     recv_sems,
 ):
@@ -254,11 +258,8 @@
     def att_halves(ref):
         return ref.at[pl.ds(0, 192)], ref.at[pl.ds(192, 192)]
 
-    def out_slot(a, b):
-        return out.at[b * NX + a]
-
     def lane_halves(ref):
-        return ref.at[:, pl.ds(0, D // 2)], ref.at[:, pl.ds(D // 2, D // 2)]
+        return ref.at[:, pl.ds(0, HALF)], ref.at[:, pl.ds(HALF, HALF)]
 
     ga = ZFirst(gate_w.at[:, pl.ds(0, MAIN)], wga)
     gb = YFirst(gb_own, wgb)
@@ -432,53 +433,118 @@
     tail = rest / (1.0 + jnp.exp(-rest)) * swapped
     lane = lax.broadcasted_iota(jnp.int32, (TOK, 2 * TAIL), 1)
     hid[:, MAIN:FP] = jnp.where(lane < TAIL, tail, 0.0).astype(BF)
+
+    own = c * NX + x
+    low, high = pl.ds(0, HALF), pl.ds(HALF, HALF)
+    chunks = [{} for _ in range(4)]
+    written = []
+
+    def groups(k):
+        if k == 3:
+            return [zm(7), zp(7), z, zm(8)]
+        return [zm(2 * k + 1), zp(2 * k + 1), zm(2 * k + 2), zp(2 * k + 2)]
+
+    def lower(k):
+        at = groups(k)
+        for i in (0, 2):
+            w = jnp.concatenate([wd[at[i]].reshape(128, FP), wd[at[i + 1]].reshape(128, FP)], axis=0)
+            term = lax.dot_general(hid[...], w, (((1,), (1,)), ((), ())), preferred_element_type=F32)
+            part[k, :, :, :, pl.ds(i * 128, 256)] = term.astype(BF).reshape(NC, NX, OWN, 256)
+        chunks[k]["pair"] = send(part.at[k, pc], pair_in.at[k], dev_p)
+
+    def fold(k):
+        g = chunks[k]
+        g["pair"].wait_recv()
+        summed[k] = (part[k, c].astype(F32) + pair_in[k].astype(F32)).astype(BF)
+        g["opp_a"] = send(summed.at[k, xo, :, low], opp_in.at[k, 0], dev_xr)
+        g["opp_b"] = send(summed.at[k, xo, :, high], opp_in.at[k, 1], dev_xl)
+        g["near_b"] = send(summed.at[k, xr, :, high], near_in.at[k, 1], dev_xr)
+        g["near_a"] = send(summed.at[k, xl, :, low], near_in.at[k, 0], dev_xl)
+
+    def pass_on(k):
+        g = chunks[k]
+        g["opp_a"].wait_recv()
+        relay[k, 0] = (opp_in[k, 0].astype(F32) + summed[k, xr, :, low].astype(F32)).astype(BF)
+        g["far_a"] = send(relay.at[k, 0], far_in.at[k, 0], dev_xr)
+        g["opp_b"].wait_recv()
+        relay[k, 1] = (opp_in[k, 1].astype(F32) + summed[k, xl, :, high].astype(F32)).astype(BF)
+        g["far_b"] = send(relay.at[k, 1], far_in.at[k, 1], dev_xl)
+
+    def slot(k):
+        return lambda a, b: shuffled.at[k, b * NX + a]
+
+    def mix(k):
+        g = chunks[k]
+        base = jnp.concatenate(
+            [carried[own, :, pl.ds(pl.multiple_of(at * 128, 128), 128)] for at in groups(k)], axis=1
+        ).astype(F32)
+        g["near_a"].wait_recv()
+        g["near_b"].wait_recv()
+        for i, name in ((0, "far_a"), (1, "far_b")):
+            g[name].wait_recv()
+            cols = pl.ds(i * HALF, HALF)
+            feed = summed[k, x, :, cols].astype(F32) + near_in[k, i].astype(F32) + far_in[k, i].astype(F32)
+            feed = feed.astype(BF).astype(F32)
+            shuffled[k, own, :, cols] = (base[:, i * HALF : (i + 1) * HALF] + 0.5 * feed).astype(BF)
+        g["out"] = x_start(shuffled.at[k, own], slot(k))
+
+    def forward(k):
+        x_forward(chunks[k]["out"], slot(k), lane_halves)
+
+    def hand_over(k):
+        x_relay(chunks[k]["out"], slot(k), lane_halves)
+
+    def write(k):
+        x_done(chunks[k]["out"])
+        for i, at in enumerate(groups(k)):
+            copy = pltpu.make_async_copy(
+                shuffled.at[k, :, :, pl.ds(i * 128, 128)],
+                out.at[:, :, pl.ds(pl.multiple_of(at * 128, 128), 128)],
+                out_sems.at[len(written)],
+            )
+            copy.start()
+            written.append(copy)
+
+    dn.done(1)
+    dn.done(2)
+    lower(0)
     dn.across(8)
-    for s in range(9):
-        dn.done(s)
-
-    def lower(n, carry):
-        w = wd[pl.ds(2 * n, 2)].reshape(256, FP)
-        term = lax.dot_general(hid[...], w, (((1,), (1,)), ((), ())), preferred_element_type=F32)
-        cols = pl.ds(pl.multiple_of(n * 256, 256), 256)
-        part[:, :, :, cols] = term.astype(BF).reshape(NC, NX, OWN, 256)
-        return carry
-
-    lax.fori_loop(0, 8, lower, 0)
-
-    to_pair = send(part.at[pc], pair_in, dev_p)
-    to_pair.wait_recv()
-
-    def fold(i, carry):
-        at = lax.rem(xo + i, NX)
-        summed[at] = (part[c, at].astype(F32) + pair_in[at].astype(F32)).astype(BF)
-        return carry
-
-    lax.fori_loop(0, 4, fold, 0)
-    half = D // 2
-    low, high = pl.ds(0, half), pl.ds(half, half)
-    opp_a = send(summed.at[xo, :, low], opp_in.at[0], dev_xr)
-    opp_b = send(summed.at[xo, :, high], opp_in.at[1], dev_xl)
-    near_b = send(summed.at[xr, :, high], near_in.at[1], dev_xr)
-    near_a = send(summed.at[xl, :, low], near_in.at[0], dev_xl)
-    opp_a.wait_recv()
-    relay[0] = (opp_in[0].astype(F32) + summed[xr, :, low].astype(F32)).astype(BF)
-    opp_b.wait_recv()
-    relay[1] = (opp_in[1].astype(F32) + summed[xl, :, high].astype(F32)).astype(BF)
-    far_a = send(relay.at[0], far_in.at[0], dev_xr)
-    far_b = send(relay.at[1], far_in.at[1], dev_xl)
-    near_a.wait_recv()
-    near_b.wait_recv()
-    own = c * NX + x
-    for i, arrived in ((0, far_a), (1, far_b)):
-        arrived.wait_recv()
-        cols = pl.ds(i * half, half)
-        feed = summed[x, :, cols].astype(F32) + near_in[i].astype(F32) + far_in[i].astype(F32)
-        feed = feed.astype(BF).astype(F32)
-        out[own, :, cols] = (carried[own, :, cols].astype(F32) + 0.5 * feed).astype(BF)
-    out_g = x_start(out.at[own], out_slot)
-    x_forward(out_g, out_slot, lane_halves)
-    x_relay(out_g, out_slot, lane_halves)
-    x_done(out_g)
+    dn.done(3)
+    dn.done(4)
+    lower(1)
+    fold(0)
+    dn.done(5)
+    dn.done(6)
+    lower(2)
+    pass_on(0)
+    fold(1)
+    dn.done(7)
+    dn.done(0)
+    dn.done(8)
+    lower(3)
+    pass_on(1)
+    fold(2)
+    mix(0)
+    fold(3)
+    pass_on(2)
+    mix(1)
+    pass_on(3)
+    forward(0)
+    mix(2)
+    forward(1)
+    hand_over(0)
+    mix(3)
+    forward(2)
+    hand_over(1)
+    write(0)
+    forward(3)
+    hand_over(2)
+    write(1)
+    hand_over(3)
+    write(2)
+    write(3)
+    for copy in written:
+        copy.wait()
     for copy in started:
         copy.wait_send()
 
@@ -504,7 +570,7 @@
         name="layer",
         out_shape=jax.ShapeDtypeStruct((8, OWN, D), BF),
         in_specs=[far] + [vmem] * 4 + [smem] + [vmem] * 5,
-        out_specs=vmem,
+        out_specs=far,
         scratch_shapes=[
             pltpu.VMEM((TOK, D), BF),
             pltpu.VMEM((TOK + 2 * WIN, HD), BF),
@@ -523,14 +589,16 @@
             pltpu.VMEM((TOK, MAIN), F32),
             pltpu.VMEM((TOK, FP), F32),
             pltpu.VMEM((TOK, FP), BF),
-            pltpu.VMEM((NC, NX, OWN, D), BF),
-            pltpu.VMEM((NX, OWN, D), BF),
-            pltpu.VMEM((NX, OWN, D), BF),
-            pltpu.VMEM((2, OWN, D // 2), BF),
-            pltpu.VMEM((2, OWN, D // 2), BF),
-            pltpu.VMEM((2, OWN, D // 2), BF),
-            pltpu.VMEM((2, OWN, D // 2), BF),
+            pltpu.VMEM((4, NC, NX, OWN, CHUNK), BF),
+            pltpu.VMEM((4, NX, OWN, CHUNK), BF),
+            pltpu.VMEM((4, NX, OWN, CHUNK), BF),
+            pltpu.VMEM((4, 2, OWN, HALF), BF),
+            pltpu.VMEM((4, 2, OWN, HALF), BF),
+            pltpu.VMEM((4, 2, OWN, HALF), BF),
+            pltpu.VMEM((4, 2, OWN, HALF), BF),
+            pltpu.VMEM((4, 8, OWN, CHUNK), BF),
             pltpu.SemaphoreType.DMA,
+            pltpu.SemaphoreType.DMA((16,)),
             pltpu.SemaphoreType.DMA((COPIES,)),
             pltpu.SemaphoreType.DMA((COPIES,)),
         ],

time: 119 us -> 116 us (0.975)
  Pallas kernels: 115 us -> 111 us
    pallas_call x1, Pallas kernels: 115 us -> 111 us  [per_device(): pl.pallas_call(kernel, name='layer', out_shape=jax.ShapeDtypeStruct((8, O...]
where the time goes in v3:
time: 116 us; the launch traced here: 115 us
  Pallas kernels  111 us (96%)
  local copies, waits for them, and re-layouts  2.73 us (2%)
    pallas_call x1, Pallas kernels, per_device(): pl.pallas_call(kernel, name='layer', out_shape=jax.ShapeDtypeStruct((8, O...  111 us
    unnamed x1, local copies, waits for them, and re-layouts  2.73 us

profile of v3, /device:TPU:1, one launch (start us, length us, event | category | flops | bytes accessed | tf_op | source)
XLA Modules:
  0.0 114.8 jit_solution(16016798906540039597)
XLA Ops:
  0.7 111.4 %layer.1 = bf16[8,48,2048]{2,1,0:T(8,128)(2,1)} custom-call(bf16[384,2048]{1,0:T(8,128)(2,1)} %stream_far.1, bf16[384,128]{1,0:T(8,128)(2,1)} %query.1, bf16[384,256]{1,0:T(8,128)(2,1)} %key.1, bf16[384,256]{1,0:T(8,128)(2,1)} %value.1, s32[3,128]{1,0:T(4,128)} %bitcast.7, f32[1]{0:T(128)S(6)} %copy.13.sink, bf16[128,2048]{1,0:T(8,128)(2,1)} %out_w.1, ...), custom_call_target="tpu_custom_call" | custom-call | tf_op jit(solution)/shard_map/layer/pallas_call | solution.py:568
  112.1 2.7 %copy.14 = bf16[384,2048]{1,0:T(8,128)(2,1)} copy(bf16[384,2048]{1,0:T(8,128)(2,1)} %bitcast.4) | data formatting | bytes 3145728

commit v4 on v3

--- a/solution.py
+++ b/solution.py
@@ -28,7 +28,7 @@
 
 
 def kernel(
-    stream_far,
+    stream,
     query,
     key,
     value,
@@ -40,7 +40,6 @@
     up_w,
     down_w,
     out,
-    stream,
     kext,
     vext,
     dsend,
@@ -65,8 +64,6 @@
     near_in,
     far_in,
     shuffled,
-    local_sem,
-    out_sems,
     send_sems,
     recv_sems,
 ):
@@ -90,8 +87,6 @@
     peers = (dev_zr, dev_zl, dev_yr, dev_yl, dev_xr, dev_xl, dev_p, dev_after, dev_before)
     for peer in peers:
         pl.semaphore_signal(barrier, inc=1, device_id=peer, device_id_type=pl.DeviceIdType.MESH)
-    stream_copy = pltpu.make_async_copy(stream_far, stream, local_sem)
-    stream_copy.start()
 
     gb_own[:, 0:MAIN] = up_w[:, 0:MAIN]
     gb_own[:, MAIN:FP] = jnp.concatenate([gate_w[:, MAIN:FFL], up_w[:, MAIN:FFL]], axis=1)
@@ -274,6 +269,7 @@
     ]
     gb.start()
     ga.start()
+    dn.start()
     ow_g = x_start(out_w, ow_slot)
     ow[x * NC + c] = out_w[...]
     gb.begin()
@@ -306,36 +302,36 @@
         attended = jnp.dot(probs, v, preferred_element_type=F32).astype(BF)
         att[x * NC + c, pl.ds(block * 128, 128), :] = attended
 
+    def rings(s):
+        ga.ring(s)
+        dn.ring(s)
+        gb.ring(s)
+
+    def across(s):
+        ga.across(s)
+        dn.across(s)
+
     attend(1)
     gb.begin_last()
     for copy in halo:
         copy.wait_recv()
     attend(0)
-    ga.ring(1)
-    gb.ring(1)
+    rings(1)
     attend(2)
-    ga.across(0)
-    ga.ring(2)
-    gb.ring(2)
+    across(0)
+    rings(2)
     att_g = x_start(att.at[x * NC + c], att_slot)
-    ga.across(1)
-    dn.start()
+    across(1)
     x_forward(ow_g, ow_slot, ow_halves)
-    ga.ring(3)
-    gb.ring(3)
+    rings(3)
     x_forward(att_g, att_slot, att_halves)
-    ga.across(2)
-    dn.ring(1)
-    ga.ring(4)
-    gb.ring(4)
+    across(2)
     x_relay(ow_g, ow_slot, ow_halves)
     x_relay(att_g, att_slot, att_halves)
-    ga.across(3)
-    dn.across(0)
-    dn.ring(2)
+    rings(4)
+    across(3)
     x_done(ow_g)
     x_done(att_g)
-    stream_copy.wait()
 
     def project(n, squares):
         cols = pl.ds(pl.multiple_of(n * 256, 256), 256)
@@ -350,8 +346,7 @@
     squares = lax.fori_loop(0, 8, project, jnp.zeros((TOK, 1), F32))
     scale = lax.rsqrt(squares / D + EPS)
 
-    ga.ring(5)
-    gb.ring(5)
+    rings(5)
 
     def normalize(n, carry):
         cols = pl.ds(pl.multiple_of(n * 256, 256), 256)
@@ -360,9 +355,7 @@
         return carry
 
     lax.fori_loop(0, 8, normalize, 0)
-    ga.across(4)
-    dn.across(1)
-    dn.ring(3)
+    across(4)
 
     def accumulate(za, zb, first):
         left = jnp.concatenate(
@@ -385,11 +378,8 @@
 
     ga.done(1)
     accumulate_tag(1, True)
-    ga.ring(6)
-    gb.ring(6)
-    ga.across(5)
-    dn.across(2)
-    dn.ring(4)
+    rings(6)
+    across(5)
     ga.done(2)
     ga.done(3)
 
@@ -398,33 +388,22 @@
         return carry
 
     lax.fori_loop(2, 4, both, 0)
-    ga.ring(7)
-    gb.ring(7)
-    ga.across(6)
-    dn.across(3)
-    dn.ring(5)
+    rings(7)
+    across(6)
     ga.done(4)
     accumulate_tag(4)
-    ga.ring(8)
-    gb.ring(8)
-    ga.across(7)
-    dn.across(4)
-    dn.ring(6)
+    rings(8)
+    across(7)
     ga.done(5)
     accumulate_tag(5)
-    ga.across(8)
-    dn.across(5)
-    dn.ring(7)
     ga.done(6)
     accumulate_tag(6)
+    across(8)
     ga.done(7)
     accumulate_tag(7)
-    dn.across(6)
-    dn.ring(8)
     ga.done(0)
     ga.done(8)
     accumulate(z, zm(8), False)
-    dn.across(7)
 
     gate, up = acc_a[...], acc_b[:, 0:MAIN]
     hid[:, 0:MAIN] = (gate / (1.0 + jnp.exp(-gate)) * up).astype(BF)
@@ -437,7 +416,6 @@
     own = c * NX + x
     low, high = pl.ds(0, HALF), pl.ds(HALF, HALF)
     chunks = [{} for _ in range(4)]
-    written = []
 
     def groups(k):
         if k == 3:
@@ -497,39 +475,29 @@
     def write(k):
         x_done(chunks[k]["out"])
         for i, at in enumerate(groups(k)):
-            copy = pltpu.make_async_copy(
-                shuffled.at[k, :, :, pl.ds(i * 128, 128)],
-                out.at[:, :, pl.ds(pl.multiple_of(at * 128, 128), 128)],
-                out_sems.at[len(written)],
-            )
-            copy.start()
-            written.append(copy)
-
-    dn.done(1)
-    dn.done(2)
+            cols = pl.ds(pl.multiple_of(at * 128, 128), 128)
+            out[:, :, cols] = shuffled[k, :, :, pl.ds(i * 128, 128)]
+
+    for i in range(1, 7):
+        dn.done(i)
     lower(0)
-    dn.across(8)
-    dn.done(3)
-    dn.done(4)
     lower(1)
     fold(0)
-    dn.done(5)
-    dn.done(6)
     lower(2)
-    pass_on(0)
     fold(1)
     dn.done(7)
     dn.done(0)
     dn.done(8)
     lower(3)
+    fold(2)
+    pass_on(0)
+    fold(3)
     pass_on(1)
-    fold(2)
     mix(0)
-    fold(3)
     pass_on(2)
     mix(1)
+    forward(0)
     pass_on(3)
-    forward(0)
     mix(2)
     forward(1)
     hand_over(0)
@@ -543,8 +511,6 @@
     hand_over(3)
     write(2)
     write(3)
-    for copy in written:
-        copy.wait()
     for copy in started:
         copy.wait_send()
 
@@ -564,15 +530,13 @@
 ):
     vmem = pl.BlockSpec(memory_space=pltpu.VMEM)
     smem = pl.BlockSpec(memory_space=pltpu.SMEM)
-    far = pl.BlockSpec(memory_space=pl.ANY)
     result = pl.pallas_call(
         kernel,
         name="layer",
         out_shape=jax.ShapeDtypeStruct((8, OWN, D), BF),
-        in_specs=[far] + [vmem] * 4 + [smem] + [vmem] * 5,
-        out_specs=far,
+        in_specs=[vmem] * 5 + [smem] + [vmem] * 5,
+        out_specs=vmem,
         scratch_shapes=[
-            pltpu.VMEM((TOK, D), BF),
             pltpu.VMEM((TOK + 2 * WIN, HD), BF),
             pltpu.VMEM((TOK + 2 * WIN, HD), BF),
             pltpu.VMEM((2, 8, 128), jnp.int32),
@@ -597,13 +561,11 @@
             pltpu.VMEM((4, 2, OWN, HALF), BF),
             pltpu.VMEM((4, 2, OWN, HALF), BF),
             pltpu.VMEM((4, 8, OWN, CHUNK), BF),
-            pltpu.SemaphoreType.DMA,
-            pltpu.SemaphoreType.DMA((16,)),
             pltpu.SemaphoreType.DMA((COPIES,)),
             pltpu.SemaphoreType.DMA((COPIES,)),
         ],
         compiler_params=pltpu.CompilerParams(
-            collective_id=0, has_side_effects=True, vmem_limit_bytes=60 * 1024 * 1024
+            collective_id=0, has_side_effects=True, vmem_limit_bytes=36 * 1024 * 1024
         ),
     )(
         stream,

time: 116 us -> 113 us (0.974)
  Pallas kernels: 111 us -> 102 us
  local copies, waits for them, and re-layouts: 2.73 us -> 10.1 us
    pallas_call x1, Pallas kernels: 111 us -> 102 us  [per_device(): pl.pallas_call(kernel, name='layer', out_shape=jax.ShapeDtypeStruct((8, O...]
    unnamed x1 -> x21, local copies, waits for them, and re-layouts: 2.73 us -> 10.1 us
where the time goes in v4:
time: 113 us
  Pallas kernels  102 us (90%)
  local copies, waits for them, and re-layouts  10.1 us (9%)
    pallas_call x1, Pallas kernels, per_device(): pl.pallas_call(kernel, name='layer', out_shape=jax.ShapeDtypeStruct((8, O...  102 us
    unnamed x21, local copies, waits for them, and re-layouts  10.1 us

profile of v4, /device:TPU:1, one launch (start us, length us, event | category | flops | bytes accessed | tf_op | source)
XLA Modules:
  0.0 112.6 jit_solution(10840446961387405610)
XLA Ops:
  0.7 0.0 copy-start
  0.7 1.4 %copy-done = bf16[384,2048]{1,0:T(8,128)(2,1)S(1)} copy-done((bf16[384,2048]{1,0:T(8,128)(2,1)S(1)}, bf16[384,2048]{1,0:T(8,128)(2,1)}, u32[]{:S(2)}) %copy-start) | copy-done | bytes 1572888
  2.1 0.0 copy-start.1
  2.1 1.0 copy-done.1
  3.1 0.0 copy-start.2
  3.1 0.9 copy-done.2
  4.0 0.0 copy-start.3
  4.0 0.9 copy-done.3
  5.0 0.0 copy-start.4
  5.0 0.9 copy-done.4
  5.9 0.0 copy-start.5
  5.9 0.8 copy-done.5
  6.7 0.0 copy-start.6
  6.7 0.8 copy-done.6
  7.4 0.0 copy-start.7
  7.5 0.8 copy-done.7
  8.2 0.0 copy-start.8
  8.2 0.7 copy-done.8
  8.9 0.0 copy-start.9
  8.9 0.7 copy-done.9
  9.6 101.8 %layer.1 = bf16[8,48,2048]{2,1,0:T(8,128)(2,1)S(1)} custom-call(bf16[384,2048]{1,0:T(8,128)(2,1)S(1)} %copy-done, bf16[384,128]{1,0:T(8,128)(2,1)S(1)} %copy-done.4, bf16[384,256]{1,0:T(8,128)(2,1)S(1)} %copy-done.2, bf16[384,256]{1,0:T(8,128)(2,1)S(1)} %copy-done.3, s32[3,128]{1,0:T(4,128)S(1)} %bitcast.7, f32[1]{0:T(128)S(6)} %copy.13.sink, ...), custom_call_target="tpu_custom_call" | custom-call | tf_op jit(solution)/shard_map/layer/pallas_call | solution.py:533
  111.4 1.1 %copy.14 = bf16[384,2048]{1,0:T(8,128)(2,1)} copy(bf16[384,2048]{1,0:T(8,128)(2,1)S(1)} %bitcast.4) | data formatting | bytes 3145728
Async XLA Ops:
  0.7 1.4 %copy-start = (bf16[384,2048]{1,0:T(8,128)(2,1)S(1)}, bf16[384,2048]{1,0:T(8,128)(2,1)}, u32[]{:S(2)}) copy-start(bf16[384,2048]{1,0:T(8,128)(2,1)} %stream.1) | copy-start | bytes 4718596
  2.1 1.0 copy-start.1
  3.1 0.9 copy-start.2
  4.0 0.9 copy-start.3
  5.0 0.9 copy-start.4
  5.9 0.8 copy-start.5
  6.7 0.8 copy-start.6
  7.4 0.8 copy-start.7
  8.2 0.7 copy-start.8
  8.9 0.7 copy-start.9

commit v5 on v4

--- a/solution.py
+++ b/solution.py
@@ -28,18 +28,29 @@
 
 
 def kernel(
+    far_stream,
+    far_query,
+    far_key,
+    far_value,
+    far_docs,
+    sink,
+    far_out_w,
+    far_gain,
+    far_gate_w,
+    far_up_w,
+    far_down_w,
+    out,
     stream,
     query,
     key,
     value,
     docs,
-    sink,
     out_w,
     gain,
     gate_w,
     up_w,
     down_w,
-    out,
+    local_sems,
     kext,
     vext,
     dsend,
@@ -88,19 +99,38 @@
     for peer in peers:
         pl.semaphore_signal(barrier, inc=1, device_id=peer, device_id_type=pl.DeviceIdType.MESH)
 
+    local = {}
+
+    def fetch(name, src, dst):
+        local[name] = pltpu.make_async_copy(src, dst, local_sems.at[len(local)])
+        local[name].start()
+
+    fetch("gate_w", far_gate_w, gate_w)
+    fetch("up_w", far_up_w, up_w)
+    fetch("down_w", far_down_w, down_w)
+    fetch("docs", far_docs, docs)
+    fetch("key", far_key, key)
+    fetch("value", far_value, value)
+    fetch("out_w", far_out_w, out_w)
+    fetch("query", far_query, query)
+    fetch("gain", far_gain, gain)
+    fetch("stream", far_stream, stream)
+    local["gate_w"].wait()
+    local["up_w"].wait()
+    local["down_w"].wait()
     gb_own[:, 0:MAIN] = up_w[:, 0:MAIN]
     gb_own[:, MAIN:FP] = jnp.concatenate([gate_w[:, MAIN:FFL], up_w[:, MAIN:FFL]], axis=1)
     dn_own[:, 0:MAIN] = down_w[:, 0:MAIN]
     dn_own[:, MAIN:FP] = jnp.concatenate([down_w[:, MAIN:FFL], jnp.zeros((32, TAIL), BF)], axis=1)
+    local["docs"].wait()
     dsend[0] = jnp.broadcast_to(docs[2:3], (8, 128))
     dsend[1] = jnp.broadcast_to(docs[0:1], (8, 128))
     group = pl.multiple_of((x // 2) * HD, HD)
     lanes = pl.ds(group, HD)
-    kext[pl.ds(128, 384), :] = key[:, lanes]
-    vext[pl.ds(128, 384), :] = value[:, lanes]
+    local["key"].wait()
+    local["value"].wait()
+    local["out_w"].wait()
     wga[z, y] = gate_w[:, 0:MAIN]
-    wgb[z, y] = gb_own[...]
-    wd[z, y] = dn_own[...]
 
     pl.semaphore_wait(barrier, len(peers))
 
@@ -272,6 +302,11 @@
     dn.start()
     ow_g = x_start(out_w, ow_slot)
     ow[x * NC + c] = out_w[...]
+    wgb[z, y] = gb_own[...]
+    wd[z, y] = dn_own[...]
+    kext[pl.ds(128, 384), :] = key[:, lanes]
+    vext[pl.ds(128, 384), :] = value[:, lanes]
+    local["query"].wait()
     gb.begin()
 
     def attend(block):
@@ -332,6 +367,9 @@
     across(3)
     x_done(ow_g)
     x_done(att_g)
+
+    local["gain"].wait()
+    local["stream"].wait()
 
     def project(n, squares):
         cols = pl.ds(pl.multiple_of(n * 256, 256), 256)
@@ -530,13 +568,25 @@
 ):
     vmem = pl.BlockSpec(memory_space=pltpu.VMEM)
     smem = pl.BlockSpec(memory_space=pltpu.SMEM)
+    far = pl.BlockSpec(memory_space=pltpu.HBM)
     result = pl.pallas_call(
         kernel,
         name="layer",
-        out_shape=jax.ShapeDtypeStruct((8, OWN, D), BF),
-        in_specs=[vmem] * 5 + [smem] + [vmem] * 5,
+        out_shape=pltpu.VMEM((8, OWN, D), BF),
+        in_specs=[far] * 5 + [smem] + [far] * 5,
         out_specs=vmem,
         scratch_shapes=[
+            pltpu.VMEM((TOK, D), BF),
+            pltpu.VMEM((TOK, HD), BF),
+            pltpu.VMEM((TOK, 2 * HD), BF),
+            pltpu.VMEM((TOK, 2 * HD), BF),
+            pltpu.VMEM((3, 128), jnp.int32),
+            pltpu.VMEM((128, D), BF),
+            pltpu.VMEM((1, D), F32),
+            pltpu.VMEM((32, FFL), BF),
+            pltpu.VMEM((32, FFL), BF),
+            pltpu.VMEM((32, FFL), BF),
+            pltpu.SemaphoreType.DMA((10,)),
             pltpu.VMEM((TOK + 2 * WIN, HD), BF),
             pltpu.VMEM((TOK + 2 * WIN, HD), BF),
             pltpu.VMEM((2, 8, 128), jnp.int32),
@@ -565,7 +615,7 @@
             pltpu.SemaphoreType.DMA((COPIES,)),
         ],
         compiler_params=pltpu.CompilerParams(
-            collective_id=0, has_side_effects=True, vmem_limit_bytes=36 * 1024 * 1024
+            collective_id=0, has_side_effects=True, vmem_limit_bytes=60 * 1024 * 1024
         ),
     )(
         stream,

time: 113 us -> 105 us (0.929)
  local copies, waits for them, and re-layouts: 10.1 us -> 1.15 us
    unnamed x21 -> x1, local copies, waits for them, and re-layouts: 10.1 us -> 1.15 us
where the time goes in v5:
time: 105 us; the launch traced here: 104 us
  Pallas kernels  102 us (97%)
  local copies, waits for them, and re-layouts  1.15 us (1%)
    pallas_call x1, Pallas kernels, per_device(): pl.pallas_call(kernel, name='layer', out_shape=pltpu.VMEM((8, OWN, D), BF...  102 us

profile of v5, /device:TPU:1, one launch (start us, length us, event | category | flops | bytes accessed | tf_op | source)
XLA Modules:
  0.0 104.2 jit_solution(9621116797687548644)
XLA Ops:
  0.7 102.4 %layer.1 = bf16[8,48,2048]{2,1,0:T(8,128)(2,1)S(1)} custom-call(bf16[384,2048]{1,0:T(8,128)(2,1)} %far_stream.1, bf16[384,128]{1,0:T(8,128)(2,1)} %far_query.1, bf16[384,256]{1,0:T(8,128)(2,1)} %far_key.1, bf16[384,256]{1,0:T(8,128)(2,1)} %far_value.1, s32[3,128]{1,0:T(4,128)} %bitcast.7, f32[1]{0:T(128)S(6)} %copy.14.sink, bf16[128,2048]{1,0:T(8,128)(2,1)} %far_out_w.1, ...), custom_call_target="tpu_custom_call" | custom-call | tf_op jit(solution)/shard_map/layer/pallas_call | solution.py:572
  103.1 1.1 %copy.13 = bf16[384,2048]{1,0:T(8,128)(2,1)} copy(bf16[384,2048]{1,0:T(8,128)(2,1)S(1)} %bitcast.4) | data formatting | bytes 3145728

commit v6 on v5

--- a/solution.py
+++ b/solution.py
@@ -289,6 +289,9 @@
     ga = ZFirst(gate_w.at[:, pl.ds(0, MAIN)], wga)
     gb = YFirst(gb_own, wgb)
     dn = ZFirst(dn_own, wd)
+    gb.start()
+    ga.start()
+    dn.start()
     halo = [
         send(key.at[pl.ds(256, 128), lanes], kext.at[pl.ds(0, 128)], dev_after),
         send(value.at[pl.ds(256, 128), lanes], vext.at[pl.ds(0, 128)], dev_after),
@@ -297,9 +300,6 @@
         send(value.at[pl.ds(0, 128), lanes], vext.at[pl.ds(512, 128)], dev_before),
         send(dsend.at[1], dext.at[1], dev_before),
     ]
-    gb.start()
-    ga.start()
-    dn.start()
     ow_g = x_start(out_w, ow_slot)
     ow[x * NC + c] = out_w[...]
     wgb[z, y] = gb_own[...]
@@ -339,12 +339,10 @@
 
     def rings(s):
         ga.ring(s)
+        ga.across(s - 1)
         dn.ring(s)
+        dn.across(s - 1)
         gb.ring(s)
-
-    def across(s):
-        ga.across(s)
-        dn.across(s)
 
     attend(1)
     gb.begin_last()
@@ -353,18 +351,14 @@
     attend(0)
     rings(1)
     attend(2)
-    across(0)
     rings(2)
     att_g = x_start(att.at[x * NC + c], att_slot)
-    across(1)
     x_forward(ow_g, ow_slot, ow_halves)
     rings(3)
     x_forward(att_g, att_slot, att_halves)
-    across(2)
     x_relay(ow_g, ow_slot, ow_halves)
     x_relay(att_g, att_slot, att_halves)
     rings(4)
-    across(3)
     x_done(ow_g)
     x_done(att_g)
 
@@ -393,7 +387,6 @@
         return carry
 
     lax.fori_loop(0, 8, normalize, 0)
-    across(4)
 
     def accumulate(za, zb, first):
         left = jnp.concatenate(
@@ -417,7 +410,6 @@
     ga.done(1)
     accumulate_tag(1, True)
     rings(6)
-    across(5)
     ga.done(2)
     ga.done(3)
 
@@ -427,16 +419,15 @@
 
     lax.fori_loop(2, 4, both, 0)
     rings(7)
-    across(6)
     ga.done(4)
     accumulate_tag(4)
     rings(8)
-    across(7)
     ga.done(5)
     accumulate_tag(5)
     ga.done(6)
     accumulate_tag(6)
-    across(8)
+    ga.across(8)
+    dn.across(8)
     ga.done(7)
     accumulate_tag(7)
     ga.done(0)

time: 105 us -> 103 us (0.981)
  Pallas kernels: 102 us -> 100 us
    pallas_call x1, Pallas kernels: 102 us -> 100 us  [per_device(): pl.pallas_call(kernel, name='layer', out_shape=pltpu.VMEM((8, OWN, D), BF...]
where the time goes in v6:
time: 103 us; the launch traced here: 102 us
  Pallas kernels  100 us (97%)
  local copies, waits for them, and re-layouts  1.15 us (1%)
    pallas_call x1, Pallas kernels, per_device(): pl.pallas_call(kernel, name='layer', out_shape=pltpu.VMEM((8, OWN, D), BF...  100 us

profile of v6, /device:TPU:1, one launch (start us, length us, event | category | flops | bytes accessed | tf_op | source)
XLA Modules:
  0.0 102.2 jit_solution(4916386944864209075)
XLA Ops:
  0.7 100.4 %layer.1 = bf16[8,48,2048]{2,1,0:T(8,128)(2,1)S(1)} custom-call(bf16[384,2048]{1,0:T(8,128)(2,1)} %far_stream.1, bf16[384,128]{1,0:T(8,128)(2,1)} %far_query.1, bf16[384,256]{1,0:T(8,128)(2,1)} %far_key.1, bf16[384,256]{1,0:T(8,128)(2,1)} %far_value.1, s32[3,128]{1,0:T(4,128)} %bitcast.7, f32[1]{0:T(128)S(6)} %copy.14.sink, bf16[128,2048]{1,0:T(8,128)(2,1)} %far_out_w.1, ...), custom_call_target="tpu_custom_call" | custom-call | tf_op jit(solution)/shard_map/layer/pallas_call | solution.py:563
  101.1 1.1 %copy.13 = bf16[384,2048]{1,0:T(8,128)(2,1)} copy(bf16[384,2048]{1,0:T(8,128)(2,1)S(1)} %bitcast.4) | data formatting | bytes 3145728

commit v7 on v6

--- a/solution.py
+++ b/solution.py
@@ -518,8 +518,8 @@
     dn.done(0)
     dn.done(8)
     lower(3)
+    pass_on(0)
     fold(2)
-    pass_on(0)
     fold(3)
     pass_on(1)
     mix(0)

time: 103 us -> 103 us (level)
  no operation moved by 1% of the time
where the time goes in v7:
time: 103 us
  Pallas kernels  101 us (98%)
  local copies, waits for them, and re-layouts  1.15 us (1%)
    pallas_call x1, Pallas kernels, per_device(): pl.pallas_call(kernel, name='layer', out_shape=pltpu.VMEM((8, OWN, D), BF...  101 us

profile of v7, /device:TPU:1, one launch (start us, length us, event | category | flops | bytes accessed | tf_op | source)
XLA Modules:
  0.0 103.0 jit_solution(9967643892787238820)
XLA Ops:
  0.7 101.2 %layer.1 = bf16[8,48,2048]{2,1,0:T(8,128)(2,1)S(1)} custom-call(bf16[384,2048]{1,0:T(8,128)(2,1)} %far_stream.1, bf16[384,128]{1,0:T(8,128)(2,1)} %far_query.1, bf16[384,256]{1,0:T(8,128)(2,1)} %far_key.1, bf16[384,256]{1,0:T(8,128)(2,1)} %far_value.1, s32[3,128]{1,0:T(4,128)} %bitcast.7, f32[1]{0:T(128)S(6)} %copy.14.sink, bf16[128,2048]{1,0:T(8,128)(2,1)} %far_out_w.1, ...), custom_call_target="tpu_custom_call" | custom-call | tf_op jit(solution)/shard_map/layer/pallas_call | solution.py:563
  101.8 1.1 %copy.13 = bf16[384,2048]{1,0:T(8,128)(2,1)} copy(bf16[384,2048]{1,0:T(8,128)(2,1)S(1)} %bitcast.4) | data formatting | bytes 3145728
